TPU v7x, 32 devices: a whole 2x2x4 slice. The times are simulated.
32 devices in a mesh: ep: 8 (over z, core), tp: 4 (over y, x).
Axes of the slice: x: 2, y: 2, z: 4, core: 2. Of those that a mesh axis runs over, the one named last changes fastest.
Arguments:
- stream: bfloat16 [128, 4096], P('ep'), may hold values from -6 to 6
- previous_state: float32 [128, 128, 4096], P('ep', None, 'tp'), may hold values from -6 to 6
- mixer_norm_gain: float32 [4096], replicated, may hold values from 0.1 to 1.9
- query_matrix: bfloat16 [4096, 2048], P('ep'), may hold values from -0.09375 to 0.09375
- key_matrix: bfloat16 [4096, 2048], P('ep'), may hold values from -0.09375 to 0.09375
- value_matrix: bfloat16 [4096, 4096], P('ep', 'tp'), may hold values from -0.09375 to 0.09375
- output_gate_weight: bfloat16 [4096, 4096], P('ep', 'tp'), may hold values from -0.09375 to 0.09375
- decay_lower_factor: bfloat16 [4096, 64], replicated, may hold values from -0.09375 to 0.09375
- decay_upper_factor: bfloat16 [64, 2048], replicated, may hold values from -3 to 3
- forgetting_boost: float32 [128, 2048], P('ep'), may hold values from 0.02 to 1.5
- head_norm_gain: float32 [256], replicated, may hold values from 0.1 to 1.9
- output_matrix: bfloat16 [4096, 4096], P('tp'), may hold values from -0.1875 to 0.1875
- mixture_norm_gain: float32 [4096], replicated, may hold values from 0.1 to 1.9
- expert_gate_weight: bfloat16 [8, 1024, 4096], P('ep', 'tp'), may hold values from -0.09375 to 0.09375
- expert_up_weight: bfloat16 [8, 1024, 4096], P('ep', 'tp'), may hold values from -0.09375 to 0.09375
- expert_down_weight: bfloat16 [8, 1024, 4096], P('ep', None, 'tp'), may hold values from -0.375 to 0.375
- expert_index_table: int32 [128, 2], P('ep'), may hold values from 0 to 7, as said below
- expert_scores_within: float32 [128, 2], P('ep'), may hold values from -6 to 6
- group_probability: float32 [128], P('ep'), may hold values from 0.3 to 1
Outputs:
- new_stream: bfloat16 [128, 4096], P('ep', 'tp')
- new_state: float32 [128, 128, 4096], P('ep', None, 'tp')
Inputs may be any that keep to these rules, and one draw needn't show every extreme that they name: `expert_index_table`: the 2 experts of a sequence are distinct and lie in one group of 2 consecutive experts. Among the 16 sequences of one index of ep (aligned blocks of rows), each expert is named at most 8 times, and in every block some experts are named exactly 8 times.
All inputs are finite; a program needn't handle non-finite values.
Results may differ from a plain program's by a relative error of at most 0.02.
Values may be sent and summed in bfloat16 or wider, within the bound.
A program may use at most 128 MiB of HBM per device.

v0:
```python
import functools

import jax
import jax.numpy as jnp
from jax import lax
from jax.experimental import pallas as pl
from jax.experimental.pallas import tpu as pltpu
from jax.sharding import PartitionSpec as P

HEAD_TOTAL = 16
KEY_CHANNELS = 128
DV = 256
GROUPS = 4
STEP = 4
COST = 20_000_000_000
VM3 = 24
F32 = jnp.float32
BF16 = jnp.bfloat16
MESH = pl.DeviceIdType.MESH

epsilon = 1e-06
forgetting_softness = 16.0


def rms_scaled(values, gain_vec):
    floats = values.astype(jnp.float32)
    scaled = floats * lax.rsqrt(jnp.mean(floats * floats, axis=-1, keepdims=True) + epsilon)
    return (scaled * gain_vec).astype(jnp.bfloat16)


def general(
    stream,
    previous_state,
    mixer_norm_gain,
    query_matrix,
    key_matrix,
    value_matrix,
    output_gate_weight,
    decay_lower_factor,
    decay_upper_factor,
    forgetting_boost,
    head_norm_gain,
    output_matrix,
    mixture_norm_gain,
    expert_gate_weight,
    expert_up_weight,
    expert_down_weight,
    expert_index_table,
    expert_scores_within,
    group_probability,
):
    seq_count, model_width = stream.shape
    value_local = previous_state.shape[2]
    head_count = max(1, value_local // DV)
    head_width = min(value_local, DV)
    tp_index = lax.axis_index("tp")
    leading_head = tp_index * value_local // DV
    value_start = tp_index * value_local % DV
    key_column_span = head_count * KEY_CHANNELS
    normed = rms_scaled(stream, mixer_norm_gain)
    own_query = lax.dynamic_slice_in_dim(
        query_matrix, leading_head * KEY_CHANNELS, key_column_span, 1
    )
    own_key = lax.dynamic_slice_in_dim(key_matrix, leading_head * KEY_CHANNELS, key_column_span, 1)
    spread = lax.all_to_all(normed, "ep", split_axis=1, concat_axis=0, tiled=True)
    joined = jnp.concatenate([own_query, own_key, value_matrix, output_gate_weight], axis=1)
    summed = lax.psum_scatter(
        jnp.dot(spread, joined, preferred_element_type=jnp.float32),
        "ep",
        scatter_dimension=0,
        tiled=True,
    )
    query_sum = summed[:, :key_column_span]
    key_sum = summed[:, key_column_span : 2 * key_column_span]
    value_sum = summed[:, 2 * key_column_span : 2 * key_column_span + value_local]
    gate_sum = summed[:, 2 * key_column_span + value_local :]
    queries = (query_sum * KEY_CHANNELS ** (-0.5)).astype(jnp.bfloat16)
    key_rows = key_sum.astype(jnp.bfloat16)
    value_rows = value_sum.astype(jnp.bfloat16)
    gate_rows = gate_sum.astype(jnp.bfloat16)
    low_rank = jnp.dot(normed, decay_lower_factor, preferred_element_type=jnp.float32).astype(
        jnp.bfloat16
    )
    local_expand_matrix = lax.dynamic_slice_in_dim(
        decay_upper_factor, leading_head * KEY_CHANNELS, key_column_span, 1
    )
    forgetting_logit = jnp.dot(low_rank, local_expand_matrix, preferred_element_type=jnp.float32)
    request_boost = lax.dynamic_slice_in_dim(
        forgetting_boost, leading_head * KEY_CHANNELS, key_column_span, 1
    )
    forgetting_lograte = jax.nn.log_sigmoid(forgetting_logit) / forgetting_softness - request_boost
    factor = (
        jnp.exp(forgetting_lograte)
        .reshape(seq_count, head_count, KEY_CHANNELS)
        .transpose(0, 2, 1)[..., None]
    )
    state_four = previous_state.reshape(seq_count, KEY_CHANNELS, head_count, head_width)
    key_part = (
        key_rows.astype(jnp.float32)
        .reshape(seq_count, head_count, KEY_CHANNELS)
        .transpose(0, 2, 1)[..., None]
    )
    value_part = value_rows.astype(jnp.float32).reshape(seq_count, 1, head_count, head_width)
    updated = factor * state_four + key_part * value_part
    query_part = (
        queries.astype(jnp.float32).reshape(seq_count, head_count, KEY_CHANNELS).transpose(0, 2, 1)
    )
    readout = jnp.einsum("skh,skhv->shv", query_part, updated, precision=lax.Precision.HIGHEST)
    square_sums = jnp.sum(readout * readout, axis=-1)
    norm_table = lax.dynamic_update_slice(
        jnp.zeros((seq_count, HEAD_TOTAL), jnp.float32), square_sums, (jnp.int32(0), leading_head)
    )
    totals = lax.psum(norm_table, "tp")
    own_totals = lax.dynamic_slice_in_dim(totals, leading_head, head_count, 1)
    mean_sq = own_totals[..., None] / DV
    own_gain = lax.dynamic_slice_in_dim(head_norm_gain, value_start, head_width, 0)
    gate_part = jax.nn.silu(
        gate_rows.astype(jnp.float32).reshape(seq_count, head_count, head_width)
    )
    gated_rows = (
        (readout * lax.rsqrt(mean_sq + epsilon) * own_gain * gate_part)
        .reshape(seq_count, value_local)
        .astype(jnp.bfloat16)
    )
    partial_out = jnp.dot(gated_rows, output_matrix, preferred_element_type=jnp.float32)
    mixer_sum = lax.psum(partial_out.astype(jnp.bfloat16), "tp").astype(jnp.float32)
    blended_tokens = (stream.astype(jnp.float32) + mixer_sum).astype(jnp.bfloat16)
    normed_two = rms_scaled(blended_tokens, mixture_norm_gain)
    ep_count = lax.axis_size("ep")
    local_experts = expert_gate_weight.shape[0]
    experts_all = ep_count * local_experts
    route_count = expert_index_table.shape[1]
    capacity = 2 * seq_count * route_count // experts_all
    slot_count = experts_all * capacity
    flat_ids = expert_index_table.reshape(seq_count * route_count)
    one_hot = (flat_ids[:, None] == jnp.arange(experts_all, dtype=jnp.int32)[None, :]).astype(
        jnp.int32
    )
    rank_in = jnp.sum(one_hot * (jnp.cumsum(one_hot, axis=0) - 1), axis=1)
    place_lookup = flat_ids * capacity + rank_in
    placing = (place_lookup[:, None] == jnp.arange(slot_count, dtype=jnp.int32)[None, :]).astype(
        jnp.float32
    )
    placing = placing.reshape(seq_count, route_count, slot_count)
    logit_exp = jnp.exp(expert_scores_within)
    weights = logit_exp / jnp.sum(logit_exp, axis=-1, keepdims=True) * group_probability[:, None]
    combine = jnp.einsum("sk,skc->sc", weights, placing, precision=lax.Precision.HIGHEST)
    dispatch = jnp.sum(placing, axis=1).astype(jnp.bfloat16)
    outgoing = jnp.einsum("sc,sd->cd", dispatch, normed_two, preferred_element_type=jnp.float32)
    outgoing = outgoing.astype(jnp.bfloat16).reshape(experts_all, capacity, model_width)
    width_local = expert_down_weight.shape[2]
    arrived = lax.all_to_all(outgoing, "ep", split_axis=0, concat_axis=0, tiled=True)
    held_slots = arrived.shape[1]
    grouped = arrived.reshape(ep_count, local_experts, held_slots, model_width)
    gate_pre = jnp.einsum(
        "sxcd,xfd->sxcf", grouped, expert_gate_weight, preferred_element_type=jnp.float32
    )
    up_pre = jnp.einsum(
        "sxcd,xfd->sxcf", grouped, expert_up_weight, preferred_element_type=jnp.float32
    )
    hidden = (jax.nn.silu(gate_pre) * up_pre).astype(jnp.bfloat16)
    outputs = jnp.einsum(
        "sxcf,xfd->sxcd",
        lax.all_gather(hidden, "tp", axis=3, tiled=True),
        expert_down_weight,
        preferred_element_type=jnp.float32,
    )
    ready_rows = outputs.astype(jnp.bfloat16).reshape(
        ep_count * local_experts, held_slots, width_local
    )
    returned = lax.all_to_all(ready_rows, "ep", split_axis=0, concat_axis=0, tiled=True)
    mixture = jnp.dot(
        combine,
        returned.reshape(slot_count, width_local).astype(jnp.float32),
        precision=lax.Precision.HIGHEST,
    )
    own_mixed = lax.dynamic_slice_in_dim(blended_tokens, tp_index * width_local, width_local, 1)
    new_stream = (own_mixed.astype(jnp.float32) + mixture).astype(jnp.bfloat16)
    return (new_stream, updated.reshape(seq_count, KEY_CHANNELS, value_local))


def greet(partners):
    barrier = pltpu.get_barrier_semaphore()
    for partner in partners:
        pl.semaphore_signal(barrier, inc=1, device_id=partner, device_id_type=MESH)
    pl.semaphore_wait(barrier, len(partners))


def send(source, target, send_sem, recv_sem, partner):
    copy = pltpu.make_async_remote_copy(
        src_ref=source,
        dst_ref=target,
        send_sem=send_sem,
        recv_sem=recv_sem,
        device_id=partner,
        device_id_type=MESH,
    )
    copy.start()
    return copy


def project_kernel(
    n,
    stream_hbm,
    gain_hbm,
    query_hbm,
    key_hbm,
    value_hbm,
    gate_hbm,
    lower_hbm,
    upper_hbm,
    boost_hbm,
    fkq_ref,
    value_ref,
    gate_ref,
    stream,
    gain,
    weights,
    lower,
    upper,
    boost,
    chunks,
    spread,
    pair_out,
    pair_in,
    own,
    plane_out,
    plane_in,
    load_sem,
    chunk_send,
    chunk_recv,
    pair_send,
    pair_recv,
    plane_send,
    plane_recv,
):
    me = lax.axis_index("ep")
    tp = lax.axis_index("tp")
    core = lax.rem(me, 2)
    row = me // 2
    rows = n // 2
    seqs = stream.shape[0]
    feats = chunks.shape[2]
    span = boost.shape[1]
    width = value_hbm.shape[1]
    columns = pl.ds(pl.multiple_of(tp * span, 128), span)
    loads = [
        pltpu.make_async_copy(query_hbm.at[:, columns], weights.at[:, pl.ds(0, span)], load_sem.at[0]),
        pltpu.make_async_copy(key_hbm.at[:, columns], weights.at[:, pl.ds(span, span)], load_sem.at[1]),
        pltpu.make_async_copy(value_hbm, weights.at[:, pl.ds(2 * span, width)], load_sem.at[2]),
        pltpu.make_async_copy(gate_hbm, weights.at[:, pl.ds(2 * span + width, width)], load_sem.at[3]),
        pltpu.make_async_copy(lower_hbm, lower, load_sem.at[4]),
        pltpu.make_async_copy(upper_hbm.at[:, columns], upper, load_sem.at[5]),
        pltpu.make_async_copy(boost_hbm.at[:, columns], boost, load_sem.at[6]),
    ]
    first = [
        pltpu.make_async_copy(stream_hbm, stream, load_sem.at[7]),
        pltpu.make_async_copy(gain_hbm, gain, load_sem.at[8]),
    ]
    for load in first + loads:
        load.start()
    greet([{"ep": lax.rem(me + d, n)} for d in range(1, n)])
    for load in first:
        load.wait()
    floats = stream[...].astype(F32)
    scale = lax.rsqrt(jnp.mean(floats * floats, axis=-1, keepdims=True) + epsilon)
    normed = (floats * scale * gain[...]).astype(BF16)
    for d in range(n):
        chunks[d] = normed[:, d * feats : (d + 1) * feats]
    sent = []
    for d in range(1, n):
        peer = lax.rem(me + d, n)
        slot = row + rows * (d % 2)
        sent.append(
            send(chunks.at[peer], spread.at[slot], chunk_send.at[d], chunk_recv.at[d], {"ep": peer})
        )
    spread[row] = chunks[me]
    for load in loads[4:]:
        load.wait()
    nt = (((1,), (1,)), ((), ()))
    low_rank = lax.dot_general(normed, lower[...], nt, preferred_element_type=F32).astype(BF16)
    logit = jnp.dot(low_rank, upper[...], preferred_element_type=F32)
    log_sig = jnp.minimum(logit, 0.0) - jnp.log1p(jnp.exp(-jnp.abs(logit)))
    factor = jnp.exp(log_sig / forgetting_softness - boost[...])
    for load in loads[:4]:
        load.wait()
    for copy in sent:
        copy.wait_recv()
    half = rows * seqs
    x = spread[...].reshape(n * seqs, feats)
    cuts = [(0, 2 * span), (2 * span, width), (2 * span + width, width)]
    partner = {"ep": me + 1 - 2 * core}
    pairs = []
    for b, (start, size) in enumerate(cuts):
        part = jnp.dot(x, weights[:, start : start + size], preferred_element_type=F32)
        pair_out[:, start : start + size] = part[half:].astype(BF16)
        own[:, :, start : start + size] = part[:half].reshape(rows, seqs, size)
        at = (slice(None), pl.ds(start, size))
        pairs.append(
            send(pair_out.at[at], pair_in.at[at], pair_send.at[b], pair_recv.at[b], partner)
        )
    planes = []
    for b, (start, size) in enumerate(cuts):
        pairs[b].wait_recv()
        both = own[:, :, start : start + size] + pair_in[:, start : start + size].astype(
            F32
        ).reshape(rows, seqs, size)
        own[:, :, start : start + size] = both
        plane_out[:, :, start : start + size] = both.astype(BF16)
        for d in range(1, rows):
            there = lax.rem(row + d, rows)
            planes.append(
                send(
                    plane_out.at[there, :, pl.ds(start, size)],
                    plane_in.at[d, :, pl.ds(start, size)],
                    plane_send.at[b, d],
                    plane_recv.at[b, d],
                    {"ep": there * 2 + core},
                )
            )
    steps = seqs // STEP
    for b, (start, size) in enumerate(cuts):
        total = own[row, :, start : start + size]
        for d in range(1, rows):
            planes[b * (rows - 1) + d - 1].wait_recv()
            total = total + plane_in[d, :, start : start + size].astype(F32)
        if b == 0:
            query = (total[:, :span] * KEY_CHANNELS ** (-0.5)).astype(BF16).astype(F32)
            key = total[:, span:].astype(BF16).astype(F32)
            for i in range(steps):
                cut = slice(i * STEP, (i + 1) * STEP)
                fkq_ref[i, 0:STEP] = factor[cut]
                fkq_ref[i, STEP : 2 * STEP] = key[cut]
                fkq_ref[i, 2 * STEP : 3 * STEP] = query[cut]
                fkq_ref[i, 3 * STEP : 4 * STEP] = query[cut]
        else:
            target = value_ref if b == 1 else gate_ref
            total = total.astype(BF16).astype(F32)
            for i in range(steps):
                target[i] = total[i * STEP : (i + 1) * STEP]
    for copy in sent + pairs + planes:
        copy.wait_send()


def state_kernel(state_ref, fkq_ref, value_ref, new_hbm, read_ref, turned, buffer, out_sem):
    seqs, _, width = state_ref.shape
    heads = width // DV
    steps = seqs // STEP

    def flush(i, slot):
        return pltpu.make_async_copy(
            buffer.at[slot], new_hbm.at[pl.ds(i * STEP, STEP)], out_sem.at[slot]
        )

    @pl.loop(0, steps)
    def _(i):
        slot = lax.rem(i, 2)

        @pl.when(i >= 2)
        def _():
            flush(i - 2, slot).wait()

        for h in range(heads):
            turned[h] = fkq_ref[i, :, h * KEY_CHANNELS : (h + 1) * KEY_CHANNELS].T
        for s in range(STEP):
            sums = []
            for h in range(heads):
                lanes = slice(h * DV, (h + 1) * DV)
                factor = turned[h, :, s : s + 1]
                key = turned[h, :, STEP + s : STEP + s + 1]
                query = turned[h, :, 2 * STEP + s : 2 * STEP + s + 1]
                updated = factor * state_ref[i * STEP + s, :, lanes] + key * value_ref[
                    i, s : s + 1, lanes
                ]
                buffer[slot, s, :, lanes] = updated
                sums.append(jnp.sum((query * updated).reshape(-1, 8, DV), axis=0))
            read_ref[i * STEP + s] = jnp.concatenate(sums, axis=1)
        flush(i, slot).start()

    for i in range(steps - 2, steps):
        flush(i, i % 2).wait()


def mixture_kernel(
    n,
    m,
    read_ref,
    rows_ref,
    head_gain_ref,
    stream_hbm,
    gain_ref,
    index_ref,
    score_ref,
    prob_ref,
    output_hbm,
    gate_hbm,
    up_hbm,
    down_hbm,
    out_ref,
    own_stream,
    w_out,
    w_gate,
    w_up,
    w_down,
    lhs,
    part_out,
    part_in,
    slots_out,
    arrived,
    hidden,
    ready,
    returned,
    load_sem,
    part_send,
    part_recv,
    slot_send,
    slot_recv,
    join_send,
    join_recv,
    swap_send,
    swap_recv,
    hid_send,
    hid_recv,
    back_send,
    back_recv,
):
    me = lax.axis_index("ep")
    tp = lax.axis_index("tp")
    seqs, width = own_stream.shape
    rows = n // 2
    capacity = slots_out.shape[1]
    others = [lax.rem(tp + d, m) for d in range(1, m)] + [tp]
    own_cut = pl.ds(pl.multiple_of(tp * width, 128), width)
    load = pltpu.make_async_copy(stream_hbm.at[:, own_cut], own_stream, load_sem.at[m + 3])
    loads = []
    for j, there in enumerate(others):
        cut = pl.ds(pl.multiple_of(there * width, 128), width)
        loads.append(pltpu.make_async_copy(output_hbm.at[:, cut], w_out.at[j], load_sem.at[j]))
    loads += [
        pltpu.make_async_copy(gate_hbm, w_gate, load_sem.at[m]),
        pltpu.make_async_copy(up_hbm, w_up, load_sem.at[m + 1]),
        pltpu.make_async_copy(down_hbm, w_down, load_sem.at[m + 2]),
    ]
    for one in loads + [load]:
        one.start()
    for i in range(seqs // STEP):
        lhs[i * STEP : (i + 1) * STEP] = rows_ref[i]
    gates = lhs[...]
    silu = gates / (1.0 + jnp.exp(-gates))
    readout = jnp.sum(read_ref[...], axis=1)
    for h in range(width // DV):
        lanes = slice(h * DV, (h + 1) * DV)
        part = readout[:, lanes]
        mean_sq = jnp.mean(part * part, axis=-1, keepdims=True)
        lhs[:, lanes] = part * lax.rsqrt(mean_sq + epsilon) * head_gain_ref[...] * silu[:, lanes]
    gated = lhs[...].astype(BF16)
    greet(
        [{"tp": there} for there in others[:-1]]
        + [{"ep": lax.rem(me + d, n)} for d in range(1, n)]
    )
    parts = []
    for j, there in enumerate(others):
        loads[j].wait()
        part = jnp.dot(gated, w_out[j], preferred_element_type=F32)
        if j < m - 1:
            part_out[j] = part.astype(BF16)
            parts.append(
                send(part_out.at[j], part_in.at[j], part_send.at[j], part_recv.at[j], {"tp": there})
            )

    index = index_ref[...]
    group = index[:, 0:1] // (n // GROUPS)
    lane = lax.broadcasted_iota(jnp.int32, (seqs, 128), 1)
    one_hot = (lane == group).astype(F32)
    earlier = lax.broadcasted_iota(jnp.int32, (seqs, seqs), 1) < lax.broadcasted_iota(
        jnp.int32, (seqs, seqs), 0
    )
    counts = jnp.dot(earlier.astype(F32), one_hot, preferred_element_type=F32)
    rank = jnp.sum(counts * one_hot, axis=1, keepdims=True).astype(jnp.int32)
    slot_lane = lax.broadcasted_iota(jnp.int32, (seqs, GROUPS * capacity), 1)
    placing = (slot_lane == group * capacity + rank).astype(F32)
    scores = jnp.exp(score_ref[...])
    weights = scores / jnp.sum(scores, axis=-1, keepdims=True) * prob_ref[...]
    back_lane = lax.broadcasted_iota(jnp.int32, (seqs, n * capacity), 1)
    combine = jnp.zeros((seqs, n * capacity), F32)
    for k in range(index.shape[1]):
        combine += jnp.where(
            back_lane == index[:, k : k + 1] * capacity + rank, weights[:, k : k + 1], 0.0
        )

    load.wait()
    total = part
    for j in range(m - 1):
        parts[j].wait_recv()
        total = total + part_in[j].astype(F32)
    mixed = (own_stream[...].astype(F32) + total).astype(BF16)
    slots = lax.dot_general(
        placing, mixed.astype(F32), (((0,), (0,)), ((), ())), preferred_element_type=F32
    )
    slots_out[...] = slots.reshape(GROUPS, capacity, width).astype(BF16)
    core = lax.rem(me, 2)
    row = me // 2
    moved = []
    for d in range(1, rows):
        there = lax.rem(row + d, rows)
        moved.append(
            send(
                slots_out.at[there],
                arrived.at[tp, core, row],
                slot_send.at[d],
                slot_recv.at[d],
                {"ep": there * 2 + core},
            )
        )
    arrived[tp, core, row] = slots_out[row]
    for copy in moved:
        copy.wait_recv()
    joins = []
    for j, there in enumerate(others[:-1]):
        joins.append(
            send(
                arrived.at[tp, core],
                arrived.at[tp, core],
                join_send.at[j],
                join_recv.at[j],
                {"tp": there},
            )
        )
    for one in loads[m:]:
        one.wait()
    swaps = []
    nt = (((1,), (1,)), ((), ()))
    tokens_held = n * capacity
    square = jnp.zeros((tokens_held, 1), F32)
    gate_pre = jnp.zeros((tokens_held, w_gate.shape[1]), F32)
    up_pre = jnp.zeros((tokens_held, w_gate.shape[1]), F32)
    origin = [tp] + [lax.rem(tp - 1 - j + m, m) for j in range(m - 1)]
    for j, t in enumerate(origin):
        if j > 0:
            joins[j - 1].wait_recv()
        swaps.append(
            send(
                arrived.at[t, core],
                arrived.at[t, core],
                swap_send.at[j],
                swap_recv.at[j],
                {"ep": me + 1 - 2 * core},
            )
        )
    for j, t in enumerate(origin):
        swaps[j].wait_recv()
        cut = pl.ds(pl.multiple_of(t * width, 128), width)
        tokens = arrived[t].astype(F32).reshape(tokens_held, width)
        square += jnp.sum(tokens * tokens, axis=-1, keepdims=True)
        scaled = (tokens * gain_ref[:, cut]).astype(BF16)
        gate_pre += lax.dot_general(scaled, w_gate[0, :, cut], nt, preferred_element_type=F32)
        up_pre += lax.dot_general(scaled, w_up[0, :, cut], nt, preferred_element_type=F32)
    scale = lax.rsqrt(square / (m * width) + epsilon)
    gate_pre *= scale
    up_pre *= scale
    inner = gate_pre.shape[1]
    hidden[tp] = (gate_pre / (1.0 + jnp.exp(-gate_pre)) * up_pre).astype(BF16)
    shared = []
    for j, there in enumerate(others[:-1]):
        shared.append(
            send(hidden.at[tp], hidden.at[tp], hid_send.at[j], hid_recv.at[j], {"tp": there})
        )
    for copy in shared:
        copy.wait_recv()
    outputs = jnp.zeros((n * capacity, width), F32)
    for t in range(m):
        outputs += jnp.dot(
            hidden[t], w_down[0, t * inner : (t + 1) * inner, :], preferred_element_type=F32
        )
    ready[...] = outputs.reshape(n, capacity, width).astype(BF16)
    backs = []
    for d in range(1, n):
        peer = lax.rem(me + d, n)
        backs.append(
            send(
                ready.at[lax.rem(peer, 2) * rows + peer // 2],
                returned.at[me],
                back_send.at[d],
                back_recv.at[d],
                {"ep": peer},
            )
        )
    returned[me] = ready[core * rows + row]
    for copy in backs:
        copy.wait_recv()
    rows = returned[...].astype(F32).reshape(n * capacity, width)
    mixture = jnp.dot(
        combine, rows, preferred_element_type=F32, precision=lax.Precision.HIGHEST
    )
    out_ref[...] = (mixed.astype(F32) + mixture).astype(BF16)
    for copy in parts + moved + joins + swaps + shared + backs:
        copy.wait_send()


def fused(
    stream,
    previous_state,
    mixer_norm_gain,
    query_matrix,
    key_matrix,
    value_matrix,
    output_gate_weight,
    decay_lower_factor,
    decay_upper_factor,
    forgetting_boost,
    head_norm_gain,
    output_matrix,
    mixture_norm_gain,
    expert_gate_weight,
    expert_up_weight,
    expert_down_weight,
    expert_index_table,
    expert_scores_within,
    group_probability,
):
    n = lax.axis_size("ep")
    m = lax.axis_size("tp")
    seqs, model = stream.shape
    width = previous_state.shape[2]
    span = width // DV * KEY_CHANNELS
    feats = query_matrix.shape[0]
    rank = decay_lower_factor.shape[1]
    steps = seqs // STEP
    total = 2 * span + 2 * width
    rows = n // 2
    half = rows * seqs
    dma = pltpu.SemaphoreType.DMA
    vmem = pl.BlockSpec(memory_space=pltpu.VMEM)
    hbm = pl.BlockSpec(memory_space=pltpu.HBM)
    fkq, values, gates = pl.pallas_call(
        functools.partial(project_kernel, n),
        name="project",
        out_shape=(
            jax.ShapeDtypeStruct((steps, 4 * STEP, span), F32),
            jax.ShapeDtypeStruct((steps, STEP, width), F32),
            jax.ShapeDtypeStruct((steps, STEP, width), F32),
        ),
        in_specs=[hbm] * 9,
        out_specs=(vmem,) * 3,
        scratch_shapes=[
            pltpu.VMEM((seqs, model), BF16),
            pltpu.VMEM((1, model), F32),
            pltpu.VMEM((feats, total), BF16),
            pltpu.VMEM((rank, model), BF16),
            pltpu.VMEM((rank, span), BF16),
            pltpu.VMEM((seqs, span), F32),
            pltpu.VMEM((n, seqs, feats), BF16),
            pltpu.VMEM((n, seqs, feats), BF16),
            pltpu.VMEM((half, total), BF16),
            pltpu.VMEM((half, total), BF16),
            pltpu.VMEM((rows, seqs, total), F32),
            pltpu.VMEM((rows, seqs, total), BF16),
            pltpu.VMEM((rows, seqs, total), BF16),
            dma((9,)),
            dma((n,)),
            dma((n,)),
            dma((3,)),
            dma((3,)),
            dma((3, rows)),
            dma((3, rows)),
        ],
        compiler_params=pltpu.CompilerParams(
            collective_id=0, has_side_effects=True, vmem_limit_bytes=12 * 2**20
        ),
        cost_estimate=pl.CostEstimate(flops=COST, bytes_accessed=3 * feats * total, transcendentals=0),
    )(
        *(pltpu.with_memory_space_constraint(a, pltpu.HBM) for a in (
            stream,
            mixer_norm_gain.reshape(1, model),
            query_matrix,
            key_matrix,
            value_matrix,
            output_gate_weight,
            decay_lower_factor.T,
            decay_upper_factor,
            forgetting_boost,
        ))
    )
    new_state, readout = pl.pallas_call(
        state_kernel,
        name="state",
        out_shape=(
            jax.ShapeDtypeStruct(previous_state.shape, F32),
            jax.ShapeDtypeStruct((seqs, 8, width), F32),
        ),
        in_specs=[vmem, vmem, vmem],
        out_specs=(hbm, vmem),
        scratch_shapes=[
            pltpu.VMEM((width // DV, KEY_CHANNELS, 4 * STEP), F32),
            pltpu.VMEM((2, STEP, KEY_CHANNELS, width), F32),
            dma((2,)),
        ],
        compiler_params=pltpu.CompilerParams(vmem_limit_bytes=10 * 2**20),
        cost_estimate=pl.CostEstimate(
            flops=COST // 4, bytes_accessed=4 * previous_state.size, transcendentals=0
        ),
    )(previous_state, fkq, values)
    inner = expert_gate_weight.shape[1]
    capacity = 2 * seqs * expert_index_table.shape[1] // n
    new_stream = pl.pallas_call(
        functools.partial(mixture_kernel, n, m),
        name="mixture",
        out_shape=jax.ShapeDtypeStruct((seqs, width), BF16),
        in_specs=[vmem] * 3 + [hbm] + [vmem] * 4 + [hbm] * 4,
        out_specs=vmem,
        scratch_shapes=[
            pltpu.VMEM((seqs, width), BF16),
            pltpu.VMEM((m, width, width), BF16),
            pltpu.VMEM(expert_gate_weight.shape, BF16),
            pltpu.VMEM(expert_up_weight.shape, BF16),
            pltpu.VMEM(expert_down_weight.shape, BF16),
            pltpu.VMEM((seqs, width), F32),
            pltpu.VMEM((m - 1, seqs, width), BF16),
            pltpu.VMEM((m - 1, seqs, width), BF16),
            pltpu.VMEM((GROUPS, capacity, width), BF16),
            pltpu.VMEM((m, 2, rows, capacity, width), BF16),
            pltpu.VMEM((m, n * capacity, inner), BF16),
            pltpu.VMEM((n, capacity, width), BF16),
            pltpu.VMEM((n, capacity, width), BF16),
            dma((m + 4,)),
            dma((m - 1,)),
            dma((m - 1,)),
            dma((rows,)),
            dma((rows,)),
            dma((m - 1,)),
            dma((m - 1,)),
            dma((m,)),
            dma((m,)),
            dma((m - 1,)),
            dma((m - 1,)),
            dma((n,)),
            dma((n,)),
        ],
        compiler_params=pltpu.CompilerParams(
            collective_id=1, has_side_effects=True, vmem_limit_bytes=VM3 * 2**20
        ),
        cost_estimate=pl.CostEstimate(flops=COST, bytes_accessed=2 * output_matrix.size, transcendentals=0),
    )(
        readout,
        gates,
        head_norm_gain.reshape(1, DV),
        stream,
        mixture_norm_gain.reshape(1, model),
        expert_index_table,
        expert_scores_within,
        group_probability.reshape(seqs, 1),
        *(
            pltpu.with_memory_space_constraint(a, pltpu.HBM)
            for a in (output_matrix, expert_gate_weight, expert_up_weight, expert_down_weight)
        ),
    )
    return (new_stream, new_state)


def on_device(*arrays):
    stream, state = arrays[0], arrays[1]
    experts_held, route_count = arrays[13].shape[0], arrays[16].shape[1]
    n = lax.axis_size("ep")
    whole_heads = state.shape[2] % DV == 0
    pair_routed = experts_held == 1 and n == GROUPS * route_count and route_count == 2
    full_tiles = stream.shape[0] % 16 == 0 and stream.shape[1] == state.shape[2] * lax.axis_size("tp")
    if whole_heads and pair_routed and full_tiles:
        return fused(*arrays)
    return general(*arrays)


def solution(mesh):
    placed = (
        P("ep", None),
        P("ep", None, "tp"),
        P(),
        P("ep", None),
        P("ep", None),
        P("ep", "tp"),
        P("ep", "tp"),
        P(),
        P(),
        P("ep", None),
        P(),
        P("tp", None),
        P(),
        P("ep", "tp", None),
        P("ep", "tp", None),
        P("ep", None, "tp"),
        P("ep", None),
        P("ep", None),
        P("ep"),
    )
    return jax.shard_map(
        on_device,
        mesh=mesh,
        in_specs=placed,
        out_specs=(P("ep", "tp"), P("ep", None, "tp")),
        check_vma=False,
    )
```

profile of v0, /device:TPU:0, one launch (start us, length us, event | category | flops | bytes accessed | tf_op | source)
XLA Modules:
  0.0 56.0 jit_solution(10152801564626851734)
XLA Ops:
  0.6 0.0 copy-start
  0.6 22.0 %project.1 = (f32[4,16,512]{2,1,0:T(8,128)S(1)}, f32[4,4,1024]{2,1,0:T(4,128)S(1)}, f32[4,4,1024]{2,1,0:T(4,128)S(1)}) custom-call(bf16[16,4096]{1,0:T(8,128)(2,1)} %stream_hbm.3, f32[1,4096]{1,0:T(1,128)} %bitcast.9, bf16[512,2048]{1,0:T(8,128)(2,1)} %query_hbm.1, bf16[512,2048]{1,0:T(8,128)(2,1)} %key_hbm.1, bf16[512,1024]{1,0:T(8,128)(2,1)} %value_hbm.1, ...), custom_call_target="tpu_custom_call" | custom-call | flops 20000000000 | bytes 4718592 | tf_op jit(solution)/shard_map/project/pallas_call | solution.py:635
  22.6 0.0 copy-done
  22.6 0.0 copy-start.4
  22.7 0.0 copy-start.5
  22.7 0.0 copy-start.6
  22.7 0.0 copy-start.1
  22.7 0.0 copy-start.2
  22.7 0.0 copy-start.3
  22.7 5.9 %state.1 = (f32[16,128,1024]{2,1,0:T(8,128)}, f32[16,8,1024]{2,1,0:T(8,128)S(1)}) custom-call(f32[16,128,1024]{2,1,0:T(8,128)S(1)} %copy-done, f32[4,16,512]{2,1,0:T(8,128)S(1)} %get-tuple-element.7.fkq_ref, f32[4,4,1024]{2,1,0:T(4,128)S(1)} %get-tuple-element.8.value_ref), custom_call_target="tpu_custom_call" | custom-call | flops 5000000000 | bytes 8388608 | tf_op jit(solution)/shard_map/state/pallas_call | solution.py:684
  28.7 0.0 copy-done.4
  28.7 0.1 copy.21.index_ref
  28.8 0.0 copy-done.5
  28.8 0.1 copy.22.score_ref
  28.8 0.0 copy-done.6
  28.8 0.1 copy.23.prob_ref
  28.9 0.0 copy-done.1
  28.9 0.0 copy-done.2
  28.9 0.0 copy-done.3
  28.9 26.4 %mixture.1 = bf16[16,1024]{1,0:T(8,128)(2,1)S(1)} custom-call(f32[16,8,1024]{2,1,0:T(8,128)S(1)} %get-tuple-element.9.read_ref, f32[4,4,1024]{2,1,0:T(4,128)S(1)} %get-tuple-element.10.rows_ref, f32[1,256]{1,0:T(1,128)S(1)} %bitcast.6, bf16[16,4096]{1,0:T(8,128)(2,1)S(1)} %copy-done.1, f32[1,4096]{1,0:T(1,128)S(1)} %bitcast.5, s32[16,2]{1,0:T(8,128)S(1)} %copy.21.index_ref, ...), custom_call_target="tpu_custom_call" | custom-call | flops 20000000000 | bytes 8388608 | tf_op jit(solution)/shard_map/mixture/pallas_call | solution.py:705
  55.4 0.6 %copy.25 = bf16[16,1024]{1,0:T(8,128)(2,1)} copy(bf16[16,1024]{1,0:T(8,128)(2,1)S(1)} %mixture.1) | data formatting | bytes 65536
Async XLA Ops:
  0.6 22.0 %copy-start = (f32[16,128,1024]{2,1,0:T(8,128)S(1)}, f32[16,128,1024]{2,1,0:T(8,128)}, u32[]{:S(2)}) copy-start(f32[16,128,1024]{2,1,0:T(8,128)} %state_ref.1) | copy-start | bytes 25165828
  22.6 6.0 %copy-start.4 = (s32[16,2]{0,1:T(2,128)S(1)}, s32[16,2]{0,1:T(2,128)}, u32[]{:S(2)}) copy-start(s32[16,2]{0,1:T(2,128)} %param.35) | copy-start | bytes 388
  22.7 6.1 %copy-start.5 = (f32[16,2]{0,1:T(2,128)S(1)}, f32[16,2]{0,1:T(2,128)}, u32[]{:S(2)}) copy-start(f32[16,2]{0,1:T(2,128)} %param.36) | copy-start | bytes 388
  22.7 6.2 %copy-start.6 = (f32[16]{0:T(128)S(1)}, f32[16]{0:T(128)}, u32[]{:S(2)}) copy-start(f32[16]{0:T(128)} %param.37) | copy-start | bytes 196
  22.7 6.3 %copy-start.1 = (bf16[16,4096]{1,0:T(8,128)(2,1)S(1)}, bf16[16,4096]{1,0:T(8,128)(2,1)}, u32[]{:S(2)}) copy-start(bf16[16,4096]{1,0:T(8,128)(2,1)} %stream_hbm.3) | copy-start | bytes 393220
  22.7 6.2 %copy-start.2 = (f32[4096]{0:T(1024)S(1)}, f32[4096]{0:T(1024)}, u32[]{:S(2)}) copy-start(f32[4096]{0:T(1024)} %param.31) | copy-start | bytes 49156
  22.7 6.2 %copy-start.3 = (f32[256]{0:T(256)S(1)}, f32[256]{0:T(256)}, u32[]{:S(2)}) copy-start(f32[256]{0:T(256)} %param.29) | copy-start | bytes 3076
where the time goes:
time: 56.2 us; the launch traced here: 56 us
  Pallas kernels  54.4 us (97%)
  local copies, waits for them, and re-layouts  0.91 us (2%)
  between operations  0.74 us (1%)
    pallas_call x1, Pallas kernels, fused(): pl.pallas_call(functools.partial(mixture_kernel, n, m), name='mixture', o...  26.4 us
    pallas_call x1, Pallas kernels, fused(): pl.pallas_call(functools.partial(project_kernel, n), name='project', out_...  22 us
    pallas_call x1, Pallas kernels, fused(): pl.pallas_call(state_kernel, name='state', out_shape=(jax.ShapeDtypeStruc...  5.94 us

commit v1 on v0

v1 whole, which is shorter than its diff:
```python
import functools

import jax
import jax.numpy as jnp
from jax import lax
from jax.experimental import pallas as pl
from jax.experimental.pallas import tpu as pltpu
from jax.sharding import PartitionSpec as P

HEAD_TOTAL = 16
KEY_CHANNELS = 128
DV = 256
GROUPS = 4
STEP = 4
COST = 20_000_000_000
VM3 = 10
F32 = jnp.float32
BF16 = jnp.bfloat16
MESH = pl.DeviceIdType.MESH

epsilon = 1e-06
forgetting_softness = 16.0


def rms_scaled(values, gain_vec):
    floats = values.astype(jnp.float32)
    scaled = floats * lax.rsqrt(jnp.mean(floats * floats, axis=-1, keepdims=True) + epsilon)
    return (scaled * gain_vec).astype(jnp.bfloat16)


def general(
    stream,
    previous_state,
    mixer_norm_gain,
    query_matrix,
    key_matrix,
    value_matrix,
    output_gate_weight,
    decay_lower_factor,
    decay_upper_factor,
    forgetting_boost,
    head_norm_gain,
    output_matrix,
    mixture_norm_gain,
    expert_gate_weight,
    expert_up_weight,
    expert_down_weight,
    expert_index_table,
    expert_scores_within,
    group_probability,
):
    seq_count, model_width = stream.shape
    value_local = previous_state.shape[2]
    head_count = max(1, value_local // DV)
    head_width = min(value_local, DV)
    tp_index = lax.axis_index("tp")
    leading_head = tp_index * value_local // DV
    value_start = tp_index * value_local % DV
    key_column_span = head_count * KEY_CHANNELS
    normed = rms_scaled(stream, mixer_norm_gain)
    own_query = lax.dynamic_slice_in_dim(
        query_matrix, leading_head * KEY_CHANNELS, key_column_span, 1
    )
    own_key = lax.dynamic_slice_in_dim(key_matrix, leading_head * KEY_CHANNELS, key_column_span, 1)
    spread = lax.all_to_all(normed, "ep", split_axis=1, concat_axis=0, tiled=True)
    joined = jnp.concatenate([own_query, own_key, value_matrix, output_gate_weight], axis=1)
    summed = lax.psum_scatter(
        jnp.dot(spread, joined, preferred_element_type=jnp.float32),
        "ep",
        scatter_dimension=0,
        tiled=True,
    )
    query_sum = summed[:, :key_column_span]
    key_sum = summed[:, key_column_span : 2 * key_column_span]
    value_sum = summed[:, 2 * key_column_span : 2 * key_column_span + value_local]
    gate_sum = summed[:, 2 * key_column_span + value_local :]
    queries = (query_sum * KEY_CHANNELS ** (-0.5)).astype(jnp.bfloat16)
    key_rows = key_sum.astype(jnp.bfloat16)
    value_rows = value_sum.astype(jnp.bfloat16)
    gate_rows = gate_sum.astype(jnp.bfloat16)
    low_rank = jnp.dot(normed, decay_lower_factor, preferred_element_type=jnp.float32).astype(
        jnp.bfloat16
    )
    local_expand_matrix = lax.dynamic_slice_in_dim(
        decay_upper_factor, leading_head * KEY_CHANNELS, key_column_span, 1
    )
    forgetting_logit = jnp.dot(low_rank, local_expand_matrix, preferred_element_type=jnp.float32)
    request_boost = lax.dynamic_slice_in_dim(
        forgetting_boost, leading_head * KEY_CHANNELS, key_column_span, 1
    )
    forgetting_lograte = jax.nn.log_sigmoid(forgetting_logit) / forgetting_softness - request_boost
    factor = (
        jnp.exp(forgetting_lograte)
        .reshape(seq_count, head_count, KEY_CHANNELS)
        .transpose(0, 2, 1)[..., None]
    )
    state_four = previous_state.reshape(seq_count, KEY_CHANNELS, head_count, head_width)
    key_part = (
        key_rows.astype(jnp.float32)
        .reshape(seq_count, head_count, KEY_CHANNELS)
        .transpose(0, 2, 1)[..., None]
    )
    value_part = value_rows.astype(jnp.float32).reshape(seq_count, 1, head_count, head_width)
    updated = factor * state_four + key_part * value_part
    query_part = (
        queries.astype(jnp.float32).reshape(seq_count, head_count, KEY_CHANNELS).transpose(0, 2, 1)
    )
    readout = jnp.einsum("skh,skhv->shv", query_part, updated, precision=lax.Precision.HIGHEST)
    square_sums = jnp.sum(readout * readout, axis=-1)
    norm_table = lax.dynamic_update_slice(
        jnp.zeros((seq_count, HEAD_TOTAL), jnp.float32), square_sums, (jnp.int32(0), leading_head)
    )
    totals = lax.psum(norm_table, "tp")
    own_totals = lax.dynamic_slice_in_dim(totals, leading_head, head_count, 1)
    mean_sq = own_totals[..., None] / DV
    own_gain = lax.dynamic_slice_in_dim(head_norm_gain, value_start, head_width, 0)
    gate_part = jax.nn.silu(
        gate_rows.astype(jnp.float32).reshape(seq_count, head_count, head_width)
    )
    gated_rows = (
        (readout * lax.rsqrt(mean_sq + epsilon) * own_gain * gate_part)
        .reshape(seq_count, value_local)
        .astype(jnp.bfloat16)
    )
    partial_out = jnp.dot(gated_rows, output_matrix, preferred_element_type=jnp.float32)
    mixer_sum = lax.psum(partial_out.astype(jnp.bfloat16), "tp").astype(jnp.float32)
    blended_tokens = (stream.astype(jnp.float32) + mixer_sum).astype(jnp.bfloat16)
    normed_two = rms_scaled(blended_tokens, mixture_norm_gain)
    ep_count = lax.axis_size("ep")
    local_experts = expert_gate_weight.shape[0]
    experts_all = ep_count * local_experts
    route_count = expert_index_table.shape[1]
    capacity = 2 * seq_count * route_count // experts_all
    slot_count = experts_all * capacity
    flat_ids = expert_index_table.reshape(seq_count * route_count)
    one_hot = (flat_ids[:, None] == jnp.arange(experts_all, dtype=jnp.int32)[None, :]).astype(
        jnp.int32
    )
    rank_in = jnp.sum(one_hot * (jnp.cumsum(one_hot, axis=0) - 1), axis=1)
    place_lookup = flat_ids * capacity + rank_in
    placing = (place_lookup[:, None] == jnp.arange(slot_count, dtype=jnp.int32)[None, :]).astype(
        jnp.float32
    )
    placing = placing.reshape(seq_count, route_count, slot_count)
    logit_exp = jnp.exp(expert_scores_within)
    weights = logit_exp / jnp.sum(logit_exp, axis=-1, keepdims=True) * group_probability[:, None]
    combine = jnp.einsum("sk,skc->sc", weights, placing, precision=lax.Precision.HIGHEST)
    dispatch = jnp.sum(placing, axis=1).astype(jnp.bfloat16)
    outgoing = jnp.einsum("sc,sd->cd", dispatch, normed_two, preferred_element_type=jnp.float32)
    outgoing = outgoing.astype(jnp.bfloat16).reshape(experts_all, capacity, model_width)
    width_local = expert_down_weight.shape[2]
    arrived = lax.all_to_all(outgoing, "ep", split_axis=0, concat_axis=0, tiled=True)
    held_slots = arrived.shape[1]
    grouped = arrived.reshape(ep_count, local_experts, held_slots, model_width)
    gate_pre = jnp.einsum(
        "sxcd,xfd->sxcf", grouped, expert_gate_weight, preferred_element_type=jnp.float32
    )
    up_pre = jnp.einsum(
        "sxcd,xfd->sxcf", grouped, expert_up_weight, preferred_element_type=jnp.float32
    )
    hidden = (jax.nn.silu(gate_pre) * up_pre).astype(jnp.bfloat16)
    outputs = jnp.einsum(
        "sxcf,xfd->sxcd",
        lax.all_gather(hidden, "tp", axis=3, tiled=True),
        expert_down_weight,
        preferred_element_type=jnp.float32,
    )
    ready_rows = outputs.astype(jnp.bfloat16).reshape(
        ep_count * local_experts, held_slots, width_local
    )
    returned = lax.all_to_all(ready_rows, "ep", split_axis=0, concat_axis=0, tiled=True)
    mixture = jnp.dot(
        combine,
        returned.reshape(slot_count, width_local).astype(jnp.float32),
        precision=lax.Precision.HIGHEST,
    )
    own_mixed = lax.dynamic_slice_in_dim(blended_tokens, tp_index * width_local, width_local, 1)
    new_stream = (own_mixed.astype(jnp.float32) + mixture).astype(jnp.bfloat16)
    return (new_stream, updated.reshape(seq_count, KEY_CHANNELS, value_local))


def greet(partners):
    barrier = pltpu.get_barrier_semaphore()
    for partner in partners:
        pl.semaphore_signal(barrier, inc=1, device_id=partner, device_id_type=MESH)
    pl.semaphore_wait(barrier, len(partners))


def send(source, target, send_sem, recv_sem, partner):
    copy = pltpu.make_async_remote_copy(
        src_ref=source,
        dst_ref=target,
        send_sem=send_sem,
        recv_sem=recv_sem,
        device_id=partner,
        device_id_type=MESH,
    )
    copy.start()
    return copy


def project_kernel(
    n,
    stream_hbm,
    gain_hbm,
    query_hbm,
    key_hbm,
    value_hbm,
    gate_hbm,
    lower_hbm,
    upper_hbm,
    boost_hbm,
    state_hbm,
    output_hbm,
    expert_gate_hbm,
    expert_up_hbm,
    expert_down_hbm,
    fkq_ref,
    value_ref,
    gate_ref,
    state_ref,
    output_ref,
    expert_gate_ref,
    expert_up_ref,
    expert_down_ref,
    stream,
    gain,
    weights,
    lower,
    upper,
    boost,
    chunks,
    spread,
    near_out,
    near_in,
    mid_out,
    mid_in,
    far_out,
    far_in,
    held,
    load_sem,
    push_send,
    push_recv,
    chunk_send,
    chunk_recv,
    near_send,
    near_recv,
    mid_send,
    mid_recv,
    far_send,
    far_recv,
):
    me = lax.axis_index("ep")
    tp = lax.axis_index("tp")
    core = lax.rem(me, 2)
    row = me // 2
    rows = n // 2
    seqs = stream.shape[0]
    feats = query_hbm.shape[0]
    span = boost.shape[1]
    width = value_hbm.shape[1]
    columns = pl.ds(pl.multiple_of(tp * span, 128), span)
    mine = pl.ds(pl.multiple_of(core * feats, 128), feats)
    sources = [query_hbm.at[:, columns], key_hbm.at[:, columns], value_hbm, gate_hbm]
    places = [
        weights.at[mine, pl.ds(0, span)],
        weights.at[mine, pl.ds(span, span)],
        weights.at[mine, pl.ds(2 * span, width)],
        weights.at[mine, pl.ds(2 * span + width, width)],
    ]
    loads = [
        pltpu.make_async_copy(source, place, load_sem.at[i])
        for i, (source, place) in enumerate(zip(sources, places))
    ]
    small = [
        pltpu.make_async_copy(lower_hbm, lower, load_sem.at[4]),
        pltpu.make_async_copy(upper_hbm.at[:, columns], upper, load_sem.at[5]),
        pltpu.make_async_copy(boost_hbm.at[:, columns], boost, load_sem.at[6]),
    ]
    first = [
        pltpu.make_async_copy(stream_hbm, stream, load_sem.at[7]),
        pltpu.make_async_copy(gain_hbm, gain, load_sem.at[8]),
    ]
    later = [
        pltpu.make_async_copy(source, place, load_sem.at[9 + i])
        for i, (source, place) in enumerate(
            [
                (state_hbm, state_ref),
                (output_hbm, output_ref),
                (expert_gate_hbm, expert_gate_ref),
                (expert_up_hbm, expert_up_ref),
                (expert_down_hbm, expert_down_ref),
            ]
        )
    ]
    partner = {"ep": me + 1 - 2 * core}
    peers = [{"ep": lax.rem(me + 2 * d, n)} for d in range(1, rows)]
    barrier = pltpu.get_barrier_semaphore()
    for peer in [partner] + peers:
        pl.semaphore_signal(barrier, inc=1, device_id=peer, device_id_type=MESH)
    for load in first + small + loads:
        load.start()
    for load in first:
        load.wait()
    floats = stream[...].astype(F32)
    scale = lax.rsqrt(jnp.mean(floats * floats, axis=-1, keepdims=True) + epsilon)
    normed = (floats * scale * gain[...]).astype(BF16)
    for d in range(rows):
        chunks[d] = normed[:, d * 2 * feats : (d + 1) * 2 * feats]
    spread[row] = chunks[row]
    pl.semaphore_wait(barrier, rows)
    side = row // 2
    outer = (row == 0) | (row == 3)
    near = row + 1 - 2 * lax.rem(row, 2)
    inner_there = 2 - side
    outer_there = 3 - 3 * side
    order = [near, inner_there, outer_there]
    inside = lax.rem(row, 2) != side
    sent = []
    back = [near, 3 - near, 3 - row]
    for j, there in enumerate(back):
        sent.append(
            send(
                chunks.at[there],
                spread.at[row],
                chunk_send.at[j],
                chunk_recv.at[row],
                {"ep": there * 2 + core},
            )
        )
    pushes = [
        send(source, place, push_send.at[i], push_recv.at[i], partner)
        for i, (source, place) in enumerate(zip(sources, places))
    ]
    for load in later:
        load.start()
    for load in small:
        load.wait()
    nt = (((1,), (1,)), ((), ()))
    low_rank = lax.dot_general(normed, lower[...], nt, preferred_element_type=F32).astype(BF16)
    logit = jnp.dot(low_rank, upper[...], preferred_element_type=F32)
    log_sig = jnp.minimum(logit, 0.0) - jnp.log1p(jnp.exp(-jnp.abs(logit)))
    factor = jnp.exp(log_sig / forgetting_softness - boost[...])
    high = factor.astype(BF16).astype(F32)
    middle = (factor - high).astype(BF16).astype(F32)
    low = factor - high - middle
    steps = seqs // STEP
    for i in range(steps):
        cut = slice(i * STEP, (i + 1) * STEP)
        fkq_ref[i, 0:STEP] = high[cut]
        fkq_ref[i, STEP : 2 * STEP] = middle[cut]
        fkq_ref[i, 2 * STEP : 3 * STEP] = low[cut]
        fkq_ref[i, 5 * STEP : 6 * STEP] = jnp.zeros_like(low[cut])
    cuts = [(0, 2 * span), (2 * span, width), (2 * span + width, width)]
    needs = [(0, 1), (2,), (3,)]
    copies = list(sent) + list(pushes)

    def cut_of(ref, b, *lead):
        return ref.at[(*lead, slice(None), pl.ds(*cuts[b]))]

    def ready(b):
        for i in needs[b]:
            loads[i].wait()
            pushes[i].wait_recv()

    def part_of(source, b):
        start, size = cuts[b]
        return jnp.dot(
            spread[source], weights[:, start : start + size], preferred_element_type=F32
        )

    def arrival(there):
        return pltpu.make_async_remote_copy(
            src_ref=chunks.at[0],
            dst_ref=spread.at[there],
            send_sem=chunk_send.at[0],
            recv_sem=chunk_recv.at[there],
            device_id=partner,
            device_id_type=MESH,
        )

    arrival(near).wait_recv()
    for b in range(3):
        ready(b)
        start, size = cuts[b]
        near_out[:, start : start + size] = part_of(near, b).astype(BF16)
        copies.append(
            send(
                cut_of(near_out, b),
                cut_of(near_in, b),
                near_send.at[b],
                near_recv.at[b],
                {"ep": near * 2 + core},
            )
        )
    arrival(inner_there).wait_recv()
    for b in range(3):
        start, size = cuts[b]
        part = part_of(inner_there, b)
        held[:, start : start + size] = part
        mid_out[:, start : start + size] = part.astype(BF16)

        @pl.when(jnp.logical_not(inside))
        def _():
            send(
                cut_of(mid_out, b),
                cut_of(mid_in, b),
                mid_send.at[b],
                mid_recv.at[b],
                {"ep": near * 2 + core},
            )

    arrival(outer_there).wait_recv()
    slot = jnp.where(inside, 0, 1)
    for b in range(3):
        start, size = cuts[b]
        far_out[:, start : start + size] = part_of(outer_there, b).astype(BF16)
        copies.append(
            send(
                cut_of(far_out, b),
                cut_of(far_in, b, slot),
                far_send.at[b],
                far_recv.at[slot, b],
                {"ep": outer_there * 2 + core},
            )
        )

    def middle_copy(b):
        return pltpu.make_async_remote_copy(
            src_ref=cut_of(mid_out, b),
            dst_ref=cut_of(far_in, b, 0),
            send_sem=mid_send.at[b],
            recv_sem=far_recv.at[0, b],
            device_id={"ep": inner_there * 2 + core},
            device_id_type=MESH,
        )

    def waiting(target, b, sem):
        return pltpu.make_async_remote_copy(
            src_ref=cut_of(mid_out, b),
            dst_ref=target,
            send_sem=mid_send.at[b],
            recv_sem=sem,
            device_id=partner,
            device_id_type=MESH,
        )

    @pl.when(inside)
    def _():
        for b in range(3):
            start, size = cuts[b]
            waiting(cut_of(mid_in, b), b, mid_recv.at[b]).wait_recv()
            merged = held[:, start : start + size] + mid_in[:, start : start + size].astype(F32)
            mid_out[:, start : start + size] = merged.astype(BF16)
            middle_copy(b).start()

    for b in range(3):
        start, size = cuts[b]
        held[:, start : start + size] = part_of(row, b)
    for b in range(3):
        start, size = cuts[b]
        waiting(cut_of(near_in, b), b, near_recv.at[b]).wait_recv()
        waiting(cut_of(far_in, b, 0), b, far_recv.at[0, b]).wait_recv()
        held[:, start : start + size] += near_in[:, start : start + size].astype(F32) + far_in[
            0, :, start : start + size
        ].astype(F32)

        @pl.when(jnp.logical_not(inside))
        def _():
            waiting(cut_of(far_in, b, 1), b, far_recv.at[1, b]).wait_recv()
            held[:, start : start + size] += far_in[1, :, start : start + size].astype(F32)

        total = held[:, start : start + size]
        if b == 0:
            query = (total[:, :span] * KEY_CHANNELS ** (-0.5)).astype(BF16).astype(F32)
            key = total[:, span:].astype(BF16).astype(F32)
            for i in range(steps):
                cut = slice(i * STEP, (i + 1) * STEP)
                fkq_ref[i, 3 * STEP : 4 * STEP] = key[cut]
                fkq_ref[i, 4 * STEP : 5 * STEP] = query[cut]
        else:
            target = value_ref if b == 1 else gate_ref
            total = total.astype(BF16).astype(F32)
            for i in range(steps):
                target[i] = total[i * STEP : (i + 1) * STEP]
    for copy in copies:
        copy.wait_send()
    for b in range(3):
        middle_copy(b).wait_send()
    for load in later:
        load.wait()


def state_kernel(state_ref, fkq_ref, value_ref, new_hbm, read_ref, spots, wide, buffer, out_sem):
    seqs, _, width = state_ref.shape
    heads = width // DV
    steps = seqs // STEP
    lines = fkq_ref.shape[1]
    line = lax.broadcasted_iota(jnp.int32, (lines, 3 * STEP * KEY_CHANNELS), 0)
    block = lax.broadcasted_iota(jnp.int32, (lines, 3 * STEP * KEY_CHANNELS), 1) // KEY_CHANNELS
    kind = jnp.maximum(line // STEP - 2, 0)
    wanted = (block // STEP == kind) & (block % STEP == line % STEP) & (line < 5 * STEP)
    spots[...] = wanted.astype(F32).astype(BF16)

    def flush(s):
        return pltpu.make_async_copy(buffer.at[s], new_hbm.at[s], out_sem.at[s])

    @pl.loop(0, steps)
    def _(i):
        for h in range(heads):
            turned = fkq_ref[i, :, h * KEY_CHANNELS : (h + 1) * KEY_CHANNELS].T.astype(BF16)
            wide[h] = jnp.dot(turned, spots[...], preferred_element_type=F32)
        for s in range(STEP):
            sums = []
            for h in range(heads):
                factor, key, query = (
                    wide[h, :, (j * STEP + s) * KEY_CHANNELS : (j * STEP + s + 1) * KEY_CHANNELS]
                    for j in range(3)
                )
                for g in range(DV // KEY_CHANNELS):
                    start = h * DV + g * KEY_CHANNELS
                    lanes = slice(start, start + KEY_CHANNELS)
                    updated = factor * state_ref[i * STEP + s, :, lanes] + key * value_ref[
                        i, s : s + 1, lanes
                    ]
                    buffer[i * STEP + s, :, lanes] = updated
                    sums.append(jnp.sum((query * updated).reshape(-1, 8, KEY_CHANNELS), axis=0))
            read_ref[i * STEP + s] = jnp.concatenate(sums, axis=1)
            flush(i * STEP + s).start()

    for s in range(seqs):
        flush(s).wait()


def mixture_kernel(
    n,
    m,
    read_ref,
    rows_ref,
    head_gain_ref,
    stream_hbm,
    gain_ref,
    index_ref,
    score_ref,
    prob_ref,
    w_out,
    w_gate,
    w_up,
    w_down,
    out_ref,
    own_stream,
    lhs,
    part_out,
    part_in,
    slots_out,
    shares_out,
    shares_in,
    arrived,
    hidden_out,
    hidden_in,
    pair_down,
    ready,
    returned,
    load_sem,
    part_send,
    part_recv,
    slot_send,
    slot_recv,
    share_send,
    share_recv,
    join_send,
    join_recv,
    swap_send,
    swap_recv,
    push_send,
    push_recv,
    hid_send,
    hid_recv,
    back_send,
    back_recv,
):
    me = lax.axis_index("ep")
    tp = lax.axis_index("tp")
    core = lax.rem(me, 2)
    row = me // 2
    rows = n // 2
    seqs, width = own_stream.shape
    capacity = slots_out.shape[1]
    half = rows * capacity
    inner = w_gate.shape[1]
    tps = [m - 1 - tp, tp + 1 - 2 * lax.rem(tp, 2), lax.rem(tp + 2, m)]
    near = row + 1 - 2 * lax.rem(row, 2)
    zs = [3 - row, 3 - near, near]
    other = me + 1 - 2 * core
    partners = (
        [{"tp": t} for t in tps]
        + [{"ep": z * 2 + core} for z in zs]
        + [{"ep": other}]
        + [{"tp": t, "ep": other} for t in tps]
    )
    barrier = pltpu.get_barrier_semaphore()
    for partner in partners:
        pl.semaphore_signal(barrier, inc=1, device_id=partner, device_id_type=MESH)
    own_cut = pl.ds(pl.multiple_of(tp * width, 128), width)
    load = pltpu.make_async_copy(stream_hbm.at[:, own_cut], own_stream, load_sem.at[0])
    load.start()
    for i in range(seqs // STEP):
        lhs[i * STEP : (i + 1) * STEP] = rows_ref[i]
    gates = lhs[...]
    silu = gates / (1.0 + jnp.exp(-gates))
    readout = jnp.sum(read_ref[...], axis=1)
    for h in range(width // DV):
        lanes = slice(h * DV, (h + 1) * DV)
        part = readout[:, lanes]
        mean_sq = jnp.mean(part * part, axis=-1, keepdims=True)
        lhs[:, lanes] = part * lax.rsqrt(mean_sq + epsilon) * head_gain_ref[...] * silu[:, lanes]
    gated = lhs[...].astype(BF16)
    done = []
    parts = []
    for j, there in enumerate(tps + [tp]):
        cut = pl.ds(pl.multiple_of(there * width, 128), width)
        part = jnp.dot(gated, w_out[:, cut], preferred_element_type=F32)
        if j == 0:
            pl.semaphore_wait(barrier, len(partners))
        if j < m - 1:
            part_out[j] = part.astype(BF16)
            parts.append(
                send(part_out.at[j], part_in.at[j], part_send.at[j], part_recv.at[j], {"tp": there})
            )
    push = send(w_down.at[0], pair_down, push_send.at[0], push_recv.at[0], {"ep": other})

    index = index_ref[...]
    group = index[0:1] // 2
    band = lax.broadcasted_iota(jnp.int32, (8, seqs), 0)
    one_hot = (band == group).astype(F32)
    earlier = lax.broadcasted_iota(jnp.int32, (seqs, seqs), 0) < lax.broadcasted_iota(
        jnp.int32, (seqs, seqs), 1
    )
    counts = jnp.dot(one_hot, earlier.astype(F32), preferred_element_type=F32)
    rank = jnp.sum(counts * one_hot, axis=0, keepdims=True).astype(jnp.int32)
    slot_line = lax.broadcasted_iota(jnp.int32, (GROUPS * capacity, seqs), 0)
    placing = (slot_line == group * capacity + rank).astype(F32)
    scores = jnp.exp(score_ref[...])
    shares = scores / jnp.sum(scores, axis=0, keepdims=True) * prob_ref[...]
    place_line = lax.broadcasted_iota(jnp.int32, (128, seqs), 0)
    table = jnp.zeros((128, seqs), F32)
    for k in range(index.shape[0]):
        table += jnp.where(place_line == lax.rem(index[k : k + 1], 2), shares[k : k + 1], 0.0)
    nt = (((1,), (1,)), ((), ()))
    shares_out[...] = lax.dot_general(
        placing, table, nt, preferred_element_type=F32, precision=lax.Precision.HIGHEST
    ).reshape(GROUPS, capacity, 128)
    placing = placing.astype(BF16)

    for z in zs:
        done.append(
            send(
                shares_out.at[z],
                shares_in.at[row],
                share_send.at[z],
                share_recv.at[row],
                {"ep": z * 2 + core},
            )
        )
    shares_in[row] = shares_out[row]
    load.wait()
    total = part + own_stream[...].astype(F32)
    for j in (1, 2, 0):
        parts[j].wait_recv()
        total = total + part_in[j].astype(F32)
    mixed = total.astype(BF16)
    slots = jnp.dot(placing, mixed, preferred_element_type=F32)
    slots_out[...] = slots.reshape(GROUPS, capacity, width).astype(BF16)
    for z in zs:
        done.append(
            send(
                slots_out.at[z],
                arrived.at[tp, core, row],
                slot_send.at[z],
                slot_recv.at[row],
                {"ep": z * 2 + core},
            )
        )
    arrived[tp, core, row] = slots_out[row]

    def swap(t, z):
        done.append(
            send(
                arrived.at[t, core, z],
                arrived.at[t, core, z],
                swap_send.at[t, z],
                swap_recv.at[t, z],
                {"ep": other},
            )
        )

    def join(z):
        for t in tps:
            done.append(
                send(
                    arrived.at[tp, core, z],
                    arrived.at[tp, core, z],
                    join_send.at[t, z],
                    join_recv.at[tp, z],
                    {"tp": t},
                )
            )
        swap(tp, z)

    def expect(target, sem):
        pltpu.make_async_remote_copy(
            src_ref=target,
            dst_ref=target,
            send_sem=sem,
            recv_sem=sem,
            device_id={"ep": other},
            device_id_type=MESH,
        ).wait_recv()

    def relay(z):
        for t in (tps[1], tps[2], tps[0]):
            expect(arrived.at[t, core, z], join_recv.at[t, z])
            swap(t, z)

    order = [row] + zs[::-1]
    join(row)
    expect(arrived.at[tp, core, order[1]], slot_recv.at[order[1]])
    join(order[1])
    expect(arrived.at[tp, core, order[2]], slot_recv.at[order[2]])
    join(order[2])
    relay(order[0])
    expect(arrived.at[tp, core, order[3]], slot_recv.at[order[3]])
    join(order[3])
    relay(order[1])
    relay(order[2])

    tokens_held = n * capacity
    square = jnp.zeros((tokens_held, 1), F32)
    gate_pre = jnp.zeros((tokens_held, inner), F32)
    up_pre = jnp.zeros((tokens_held, inner), F32)
    for j, t in enumerate([tp, tps[1], tps[2], tps[0]]):
        if j == 1:
            relay(order[3])
        for z in order:
            expect(arrived.at[t, 1 - core, z], swap_recv.at[t, z])
        cut = pl.ds(pl.multiple_of(t * width, 128), width)
        tokens = arrived[t].astype(F32).reshape(tokens_held, width)
        square += jnp.sum(tokens * tokens, axis=-1, keepdims=True)
        scaled = (tokens * gain_ref[:, cut]).astype(BF16)
        gate_pre += lax.dot_general(scaled, w_gate[0, :, cut], nt, preferred_element_type=F32)
        up_pre += lax.dot_general(scaled, w_up[0, :, cut], nt, preferred_element_type=F32)
    scale = lax.rsqrt(square / (m * width) + epsilon)
    gate_pre *= scale
    up_pre *= scale
    hidden_out[...] = (
        (gate_pre / (1.0 + jnp.exp(-gate_pre)) * up_pre).astype(BF16).reshape(2, half, inner)
    )
    for j, t in enumerate(tps):
        for c in range(2):
            done.append(
                send(
                    hidden_out.at[c],
                    hidden_in.at[core, tp],
                    hid_send.at[2 * j + c],
                    hid_recv.at[core, tp],
                    {"tp": t, "ep": row * 2 + c},
                )
            )
    done.append(
        send(
            hidden_out.at[1 - core],
            hidden_in.at[core, tp],
            hid_send.at[2 * m - 2],
            hid_recv.at[core, tp],
            {"ep": other},
        )
    )
    hidden_in[core, tp] = hidden_out[core]
    push.wait_recv()
    own_sum = jnp.zeros((half, width), F32)
    pair_sum = jnp.zeros((half, width), F32)
    for j, t in enumerate([tp, tps[1], tps[2], tps[0]]):
        lines = pl.ds(pl.multiple_of(t * inner, 128), inner)
        if j > 0:
            expect(hidden_in.at[core, t], hid_recv.at[core, t])
        own_sum += jnp.dot(hidden_in[core, t], w_down[0, lines, :], preferred_element_type=F32)
        expect(hidden_in.at[1 - core, t], hid_recv.at[1 - core, t])
        pair_sum += jnp.dot(hidden_in[1 - core, t], pair_down[lines, :], preferred_element_type=F32)
    for z in zs:
        expect(shares_in.at[z], share_recv.at[z])
    share = shares_in[...].reshape(half, 128)
    which = lax.broadcasted_iota(jnp.int32, (half, 128), 1)
    own_share = jnp.sum(jnp.where(which == core, share, 0.0), axis=1, keepdims=True)
    pair_share = jnp.sum(jnp.where(which == 1 - core, share, 0.0), axis=1, keepdims=True)
    outputs = own_share * own_sum.astype(BF16).astype(F32) + pair_share * pair_sum.astype(
        BF16
    ).astype(F32)
    ready[...] = outputs.reshape(rows, capacity, width).astype(BF16)
    for z in zs:
        done.append(
            send(
                ready.at[z],
                returned.at[row],
                back_send.at[z],
                back_recv.at[row],
                {"ep": z * 2 + core},
            )
        )
    returned[row] = ready[row]
    for z in zs[::-1]:
        expect(returned.at[z], back_recv.at[z])
    mixture = lax.dot_general(
        placing,
        returned[...].reshape(half, width),
        (((0,), (0,)), ((), ())),
        preferred_element_type=F32,
    )
    out_ref[...] = (mixed.astype(F32) + mixture).astype(BF16)
    for copy in parts + done + [push]:
        copy.wait_send()


def fused(
    stream,
    previous_state,
    mixer_norm_gain,
    query_matrix,
    key_matrix,
    value_matrix,
    output_gate_weight,
    decay_lower_factor,
    decay_upper_factor,
    forgetting_boost,
    head_norm_gain,
    output_matrix,
    mixture_norm_gain,
    expert_gate_weight,
    expert_up_weight,
    expert_down_weight,
    expert_index_table,
    expert_scores_within,
    group_probability,
):
    n = lax.axis_size("ep")
    m = lax.axis_size("tp")
    seqs, model = stream.shape
    width = previous_state.shape[2]
    span = width // DV * KEY_CHANNELS
    feats = query_matrix.shape[0]
    rank = decay_lower_factor.shape[1]
    steps = seqs // STEP
    total = 2 * span + 2 * width
    rows = n // 2
    dma = pltpu.SemaphoreType.DMA
    vmem = pl.BlockSpec(memory_space=pltpu.VMEM)
    hbm = pl.BlockSpec(memory_space=pltpu.HBM)
    ahead = (
        previous_state,
        output_matrix,
        expert_gate_weight,
        expert_up_weight,
        expert_down_weight,
    )
    fkq, values, gates, *held = pl.pallas_call(
        functools.partial(project_kernel, n),
        name="project",
        out_shape=(
            jax.ShapeDtypeStruct((steps, 6 * STEP, span), F32),
            jax.ShapeDtypeStruct((steps, STEP, width), F32),
            jax.ShapeDtypeStruct((steps, STEP, width), F32),
            *(pltpu.VMEM(a.shape, a.dtype) for a in ahead),
        ),
        in_specs=[hbm] * (9 + len(ahead)),
        out_specs=(vmem,) * (3 + len(ahead)),
        scratch_shapes=[
            pltpu.VMEM((seqs, model), BF16),
            pltpu.VMEM((1, model), F32),
            pltpu.VMEM((2 * feats, total), BF16),
            pltpu.VMEM((rank, model), BF16),
            pltpu.VMEM((rank, span), BF16),
            pltpu.VMEM((seqs, span), F32),
            pltpu.VMEM((rows, seqs, 2 * feats), BF16),
            pltpu.VMEM((rows, seqs, 2 * feats), BF16),
            pltpu.VMEM((seqs, total), BF16),
            pltpu.VMEM((seqs, total), BF16),
            pltpu.VMEM((seqs, total), BF16),
            pltpu.VMEM((seqs, total), BF16),
            pltpu.VMEM((seqs, total), BF16),
            pltpu.VMEM((2, seqs, total), BF16),
            pltpu.VMEM((seqs, total), F32),
            dma((14,)),
            dma((4,)),
            dma((4,)),
            dma((rows,)),
            dma((rows,)),
            dma((3,)),
            dma((3,)),
            dma((3,)),
            dma((3,)),
            dma((3,)),
            dma((2, 3)),
        ],
        compiler_params=pltpu.CompilerParams(
            collective_id=0, has_side_effects=True, vmem_limit_bytes=12 * 2**20
        ),
        cost_estimate=pl.CostEstimate(flops=COST, bytes_accessed=3 * feats * total, transcendentals=0),
    )(
        *(pltpu.with_memory_space_constraint(a, pltpu.HBM) for a in (
            stream,
            mixer_norm_gain.reshape(1, model),
            query_matrix,
            key_matrix,
            value_matrix,
            output_gate_weight,
            decay_lower_factor.T,
            decay_upper_factor,
            forgetting_boost,
            *ahead,
        ))
    )
    previous_state, output_matrix, expert_gate_weight, expert_up_weight, expert_down_weight = held
    new_state, readout = pl.pallas_call(
        state_kernel,
        name="state",
        out_shape=(
            jax.ShapeDtypeStruct(previous_state.shape, F32),
            jax.ShapeDtypeStruct((seqs, 8, width), F32),
        ),
        in_specs=[vmem, vmem, vmem],
        out_specs=(hbm, vmem),
        scratch_shapes=[
            pltpu.VMEM((6 * STEP, 3 * STEP * KEY_CHANNELS), BF16),
            pltpu.VMEM((width // DV, KEY_CHANNELS, 3 * STEP * KEY_CHANNELS), F32),
            pltpu.VMEM(previous_state.shape, F32),
            dma((seqs,)),
        ],
        compiler_params=pltpu.CompilerParams(vmem_limit_bytes=14 * 2**20),
        cost_estimate=pl.CostEstimate(
            flops=COST // 4, bytes_accessed=4 * previous_state.size, transcendentals=0
        ),
    )(previous_state, fkq, values)
    inner = expert_gate_weight.shape[1]
    capacity = 2 * seqs * expert_index_table.shape[1] // n
    new_stream = pl.pallas_call(
        functools.partial(mixture_kernel, n, m),
        name="mixture",
        out_shape=jax.ShapeDtypeStruct((seqs, width), BF16),
        in_specs=[vmem] * 3 + [hbm] + [vmem] * 8,
        out_specs=vmem,
        scratch_shapes=[
            pltpu.VMEM((seqs, width), BF16),
            pltpu.VMEM((seqs, width), F32),
            pltpu.VMEM((m - 1, seqs, width), BF16),
            pltpu.VMEM((m - 1, seqs, width), BF16),
            pltpu.VMEM((GROUPS, capacity, width), BF16),
            pltpu.VMEM((GROUPS, capacity, 128), F32),
            pltpu.VMEM((GROUPS, capacity, 128), F32),
            pltpu.VMEM((m, 2, rows, capacity, width), BF16),
            pltpu.VMEM((2, rows * capacity, inner), BF16),
            pltpu.VMEM((2, m, rows * capacity, inner), BF16),
            pltpu.VMEM(expert_down_weight.shape[1:], BF16),
            pltpu.VMEM((rows, capacity, width), BF16),
            pltpu.VMEM((rows, capacity, width), BF16),
            dma((1,)),
            dma((m - 1,)),
            dma((m - 1,)),
            dma((rows,)),
            dma((rows,)),
            dma((rows,)),
            dma((rows,)),
            dma((m, rows)),
            dma((m, rows)),
            dma((m, rows)),
            dma((m, rows)),
            dma((1,)),
            dma((1,)),
            dma((2 * m - 1,)),
            dma((2, m)),
            dma((rows,)),
            dma((rows,)),
        ],
        compiler_params=pltpu.CompilerParams(
            collective_id=1, has_side_effects=True, vmem_limit_bytes=VM3 * 2**20
        ),
        cost_estimate=pl.CostEstimate(flops=COST, bytes_accessed=2 * output_matrix.size, transcendentals=0),
    )(
        readout,
        gates,
        head_norm_gain.reshape(1, DV),
        stream,
        mixture_norm_gain.reshape(1, model),
        expert_index_table.T,
        expert_scores_within.T,
        group_probability.reshape(1, seqs),
        output_matrix,
        expert_gate_weight,
        expert_up_weight,
        expert_down_weight,
    )
    return (new_stream, new_state)


def on_device(*arrays):
    stream, state = arrays[0], arrays[1]
    experts_held, route_count = arrays[13].shape[0], arrays[16].shape[1]
    n = lax.axis_size("ep")
    whole_heads = state.shape[2] % DV == 0
    pair_routed = experts_held == 1 and n == GROUPS * route_count and route_count == 2
    boxed = n == 8 and lax.axis_size("tp") == 4
    full_tiles = stream.shape[0] % 16 == 0 and stream.shape[1] == state.shape[2] * lax.axis_size("tp")
    if whole_heads and pair_routed and full_tiles and boxed:
        return fused(*arrays)
    return general(*arrays)


def solution(mesh):
    placed = (
        P("ep", None),
        P("ep", None, "tp"),
        P(),
        P("ep", None),
        P("ep", None),
        P("ep", "tp"),
        P("ep", "tp"),
        P(),
        P(),
        P("ep", None),
        P(),
        P("tp", None),
        P(),
        P("ep", "tp", None),
        P("ep", "tp", None),
        P("ep", None, "tp"),
        P("ep", None),
        P("ep", None),
        P("ep"),
    )
    return jax.shard_map(
        on_device,
        mesh=mesh,
        in_specs=placed,
        out_specs=(P("ep", "tp"), P("ep", None, "tp")),
        check_vma=False,
    )
```

time: 56.2 us -> 51.7 us (0.920)
  Pallas kernels: 54.4 us -> 50.2 us
    pallas_call x1, Pallas kernels: 22 us -> 18.9 us  [fused(): pl.pallas_call(functools.partial(project_kernel, n), name='project', out_...]
    pallas_call x1, Pallas kernels: 5.94 us -> 4.71 us  [fused(): pl.pallas_call(state_kernel, name='state', out_shape=(jax.ShapeDtypeStruc...]
where the time goes in v1:
time: 51.7 us; the launch traced here: 51.6 us
  Pallas kernels  50.2 us (97%)
  between operations  0.75 us (1%)
  local copies, waits for them, and re-layouts  0.66 us (1%)
    pallas_call x1, Pallas kernels, fused(): pl.pallas_call(functools.partial(mixture_kernel, n, m), name='mixture', o...  26.6 us
    pallas_call x1, Pallas kernels, fused(): pl.pallas_call(functools.partial(project_kernel, n), name='project', out_...  18.9 us
    pallas_call x1, Pallas kernels, fused(): pl.pallas_call(state_kernel, name='state', out_shape=(jax.ShapeDtypeStruc...  4.71 us

profile of v1, /device:TPU:0, one launch (start us, length us, event | category | flops | bytes accessed | tf_op | source)
XLA Modules:
  0.0 51.6 jit_solution(15232721675894592052)
XLA Ops:
  0.6 18.9 %project.1 = (f32[4,24,512]{2,1,0:T(8,128)S(1)}, f32[4,4,1024]{2,1,0:T(4,128)S(1)}, f32[4,4,1024]{2,1,0:T(4,128)S(1)}, f32[16,128,1024]{2,1,0:T(8,128)S(1)}, bf1...) custom-call(bf16[16,4096]{1,0:T(8,128)(2,1)} %stream_hbm.3, ...), custom_call_target="tpu_custom_call" | custom-call | flops 20000000000 | bytes 4718592 | tf_op jit(solution)/shard_map/project/pallas_call | solution.py:864
  19.5 0.0 copy-start
  19.5 0.0 copy-start.1
  19.6 0.0 copy-start.2
  19.6 0.0 copy-start.3
  19.6 0.0 copy-start.4
  19.6 0.0 copy-start.5
  19.6 4.7 %state.1 = (f32[16,128,1024]{2,1,0:T(8,128)}, f32[16,8,1024]{2,1,0:T(8,128)S(1)}) custom-call(f32[16,128,1024]{2,1,0:T(8,128)S(1)} %get-tuple-element.12.state_ref, f32[4,24,512]{2,1,0:T(8,128)S(1)} %get-tuple-element.13.fkq_ref, f32[4,4,1024]{2,1,0:T(4,128)S(1)} %get-tuple-element.14.value_ref), custom_call_target="tpu_custom_call" | custom-call | flops 5000000000 | bytes 8388608 | tf_op jit(solution)/shard_map/state/pallas_call | solution.py:922
  24.3 0.0 copy-done
  24.3 0.0 copy-done.1
  24.3 0.0 copy-done.2
  24.3 0.0 copy-done.3
  24.4 0.0 copy-done.4
  24.4 0.0 copy-done.5
  24.4 26.6 %mixture.1 = bf16[16,1024]{1,0:T(8,128)(2,1)S(1)} custom-call(f32[16,8,1024]{2,1,0:T(8,128)S(1)} %get-tuple-element.15.read_ref, f32[4,4,1024]{2,1,0:T(4,128)S(1)} %get-tuple-element.16.rows_ref, f32[1,256]{1,0:T(1,128)S(1)} %bitcast.8, bf16[16,4096]{1,0:T(8,128)(2,1)S(1)} %copy-done, f32[1,4096]{1,0:T(1,128)S(1)} %bitcast.7, s32[2,16]{1,0:T(2,128)S(1)} %bitcast.9, ...), custom_call_target="tpu_custom_call" | custom-call | flops 20000000000 | bytes 8388608 | tf_op jit(solution)/shard_map/mixture/pallas_call | solution.py:944
  51.0 0.6 %copy.22 = bf16[16,1024]{1,0:T(8,128)(2,1)} copy(bf16[16,1024]{1,0:T(8,128)(2,1)S(1)} %mixture.1) | data formatting | bytes 65536
Async XLA Ops:
  19.5 4.8 %copy-start = (bf16[16,4096]{1,0:T(8,128)(2,1)S(1)}, bf16[16,4096]{1,0:T(8,128)(2,1)}, u32[]{:S(2)}) copy-start(bf16[16,4096]{1,0:T(8,128)(2,1)} %stream_hbm.3) | copy-start | bytes 393220
  19.5 4.8 %copy-start.1 = (f32[4096]{0:T(1024)S(1)}, f32[4096]{0:T(1024)}, u32[]{:S(2)}) copy-start(f32[4096]{0:T(1024)} %param.31) | copy-start | bytes 49156
  19.6 4.8 %copy-start.2 = (f32[256]{0:T(256)S(1)}, f32[256]{0:T(256)}, u32[]{:S(2)}) copy-start(f32[256]{0:T(256)} %param.29) | copy-start | bytes 3076
  19.6 4.8 %copy-start.3 = (s32[16,2]{0,1:T(2,128)S(1)}, s32[16,2]{0,1:T(2,128)}, u32[]{:S(2)}) copy-start(s32[16,2]{0,1:T(2,128)} %param.35) | copy-start | bytes 388
  19.6 4.8 %copy-start.4 = (f32[16,2]{0,1:T(2,128)S(1)}, f32[16,2]{0,1:T(2,128)}, u32[]{:S(2)}) copy-start(f32[16,2]{0,1:T(2,128)} %param.36) | copy-start | bytes 388
  19.6 4.8 %copy-start.5 = (f32[16]{0:T(128)S(1)}, f32[16]{0:T(128)}, u32[]{:S(2)}) copy-start(f32[16]{0:T(128)} %param.37) | copy-start | bytes 196

commit v2 on v1

--- a/solution.py
+++ b/solution.py
@@ -13,7 +13,7 @@
 GROUPS = 4
 STEP = 4
 COST = 20_000_000_000
-VM3 = 10
+GRANT = 40
 F32 = jnp.float32
 BF16 = jnp.bfloat16
 MESH = pl.DeviceIdType.MESH
@@ -179,13 +179,6 @@
     return (new_stream, updated.reshape(seq_count, KEY_CHANNELS, value_local))
 
 
-def greet(partners):
-    barrier = pltpu.get_barrier_semaphore()
-    for partner in partners:
-        pl.semaphore_signal(barrier, inc=1, device_id=partner, device_id_type=MESH)
-    pl.semaphore_wait(barrier, len(partners))
-
-
 def send(source, target, send_sem, recv_sem, partner):
     copy = pltpu.make_async_remote_copy(
         src_ref=source,
@@ -199,8 +192,9 @@
     return copy
 
 
-def project_kernel(
+def layer_kernel(
     n,
+    m,
     stream_hbm,
     gain_hbm,
     query_hbm,
@@ -210,25 +204,34 @@
     lower_hbm,
     upper_hbm,
     boost_hbm,
+    head_gain_hbm,
+    gain_two_hbm,
+    index_hbm,
+    score_hbm,
+    prob_hbm,
     state_hbm,
     output_hbm,
     expert_gate_hbm,
     expert_up_hbm,
     expert_down_hbm,
-    fkq_ref,
-    value_ref,
-    gate_ref,
     state_ref,
-    output_ref,
-    expert_gate_ref,
-    expert_up_ref,
-    expert_down_ref,
+    out_ref,
     stream,
     gain,
     weights,
     lower,
     upper,
     boost,
+    head_gain_ref,
+    gain_ref,
+    index_ref,
+    score_ref,
+    prob_ref,
+    w_out,
+    w_gate,
+    w_up,
+    w_down,
+    pair_down,
     chunks,
     spread,
     near_out,
@@ -238,6 +241,22 @@
     far_out,
     far_in,
     held,
+    lines,
+    turned,
+    spots,
+    wide,
+    values,
+    read,
+    part_out,
+    part_in,
+    slots_out,
+    shares_out,
+    shares_in,
+    arrived,
+    hidden_out,
+    hidden_in,
+    ready,
+    returned,
     load_sem,
     push_send,
     push_recv,
@@ -249,6 +268,20 @@
     mid_recv,
     far_send,
     far_recv,
+    part_send,
+    part_recv,
+    slot_send,
+    slot_recv,
+    share_send,
+    share_recv,
+    join_send,
+    join_recv,
+    swap_send,
+    swap_recv,
+    hid_send,
+    hid_recv,
+    back_send,
+    back_recv,
 ):
     me = lax.axis_index("ep")
     tp = lax.axis_index("tp")
@@ -259,6 +292,31 @@
     feats = query_hbm.shape[0]
     span = boost.shape[1]
     width = value_hbm.shape[1]
+    heads = width // DV
+    steps = seqs // STEP
+    capacity = slots_out.shape[1]
+    half = rows * capacity
+    inner = w_gate.shape[1]
+    nt = (((1,), (1,)), ((), ()))
+    side = row // 2
+    inside = lax.rem(row, 2) != side
+    near = row + 1 - 2 * lax.rem(row, 2)
+    inner_there = 2 - side
+    outer_there = 3 - 3 * side
+    other = me + 1 - 2 * core
+    partner = {"ep": other}
+    zs = [3 - row, 3 - near, near]
+    tps = [m - 1 - tp, tp + 1 - 2 * lax.rem(tp, 2), lax.rem(tp + 2, m)]
+    partners = (
+        [partner]
+        + [{"ep": z * 2 + core} for z in zs]
+        + [{"tp": t} for t in tps]
+        + [{"tp": t, "ep": other} for t in tps]
+    )
+    barrier = pltpu.get_barrier_semaphore()
+    for there in partners:
+        pl.semaphore_signal(barrier, inc=1, device_id=there, device_id_type=MESH)
+
     columns = pl.ds(pl.multiple_of(tp * span, 128), span)
     mine = pl.ds(pl.multiple_of(core * feats, 128), feats)
     sources = [query_hbm.at[:, columns], key_hbm.at[:, columns], value_hbm, gate_hbm]
@@ -268,39 +326,36 @@
         weights.at[mine, pl.ds(2 * span, width)],
         weights.at[mine, pl.ds(2 * span + width, width)],
     ]
-    loads = [
+    pairs = [
+        (stream_hbm, stream),
+        (gain_hbm, gain),
+        (lower_hbm, lower),
+        (upper_hbm.at[:, columns], upper),
+        (boost_hbm.at[:, columns], boost),
+        *zip(sources, places),
+        (head_gain_hbm, head_gain_ref),
+        (gain_two_hbm, gain_ref),
+        (index_hbm, index_ref),
+        (score_hbm, score_ref),
+        (prob_hbm, prob_ref),
+        (state_hbm, state_ref),
+        (output_hbm, w_out),
+        (expert_gate_hbm, w_gate),
+        (expert_up_hbm, w_up),
+        (expert_down_hbm, w_down),
+    ]
+    copies = [
         pltpu.make_async_copy(source, place, load_sem.at[i])
-        for i, (source, place) in enumerate(zip(sources, places))
+        for i, (source, place) in enumerate(pairs)
     ]
-    small = [
-        pltpu.make_async_copy(lower_hbm, lower, load_sem.at[4]),
-        pltpu.make_async_copy(upper_hbm.at[:, columns], upper, load_sem.at[5]),
-        pltpu.make_async_copy(boost_hbm.at[:, columns], boost, load_sem.at[6]),
-    ]
-    first = [
-        pltpu.make_async_copy(stream_hbm, stream, load_sem.at[7]),
-        pltpu.make_async_copy(gain_hbm, gain, load_sem.at[8]),
-    ]
-    later = [
-        pltpu.make_async_copy(source, place, load_sem.at[9 + i])
-        for i, (source, place) in enumerate(
-            [
-                (state_hbm, state_ref),
-                (output_hbm, output_ref),
-                (expert_gate_hbm, expert_gate_ref),
-                (expert_up_hbm, expert_up_ref),
-                (expert_down_hbm, expert_down_ref),
-            ]
-        )
-    ]
-    partner = {"ep": me + 1 - 2 * core}
-    peers = [{"ep": lax.rem(me + 2 * d, n)} for d in range(1, rows)]
-    barrier = pltpu.get_barrier_semaphore()
-    for peer in [partner] + peers:
-        pl.semaphore_signal(barrier, inc=1, device_id=peer, device_id_type=MESH)
-    for load in first + small + loads:
+    loads = copies[5:9]
+    tables = copies[9:14]
+    state_load, out_load = copies[14:16]
+    expert_loads = copies[16:]
+    for load in copies[:14]:
         load.start()
-    for load in first:
+    done = []
+    for load in copies[:2]:
         load.wait()
     floats = stream[...].astype(F32)
     scale = lax.rsqrt(jnp.mean(floats * floats, axis=-1, keepdims=True) + epsilon)
@@ -308,18 +363,9 @@
     for d in range(rows):
         chunks[d] = normed[:, d * 2 * feats : (d + 1) * 2 * feats]
     spread[row] = chunks[row]
-    pl.semaphore_wait(barrier, rows)
-    side = row // 2
-    outer = (row == 0) | (row == 3)
-    near = row + 1 - 2 * lax.rem(row, 2)
-    inner_there = 2 - side
-    outer_there = 3 - 3 * side
-    order = [near, inner_there, outer_there]
-    inside = lax.rem(row, 2) != side
-    sent = []
-    back = [near, 3 - near, 3 - row]
-    for j, there in enumerate(back):
-        sent.append(
+    pl.semaphore_wait(barrier, len(partners))
+    for j, there in enumerate([near, 3 - near, 3 - row]):
+        done.append(
             send(
                 chunks.at[there],
                 spread.at[row],
@@ -332,33 +378,50 @@
         send(source, place, push_send.at[i], push_recv.at[i], partner)
         for i, (source, place) in enumerate(zip(sources, places))
     ]
-    for load in later:
-        load.start()
-    for load in small:
+    for load in copies[2:5]:
         load.wait()
-    nt = (((1,), (1,)), ((), ()))
     low_rank = lax.dot_general(normed, lower[...], nt, preferred_element_type=F32).astype(BF16)
     logit = jnp.dot(low_rank, upper[...], preferred_element_type=F32)
     log_sig = jnp.minimum(logit, 0.0) - jnp.log1p(jnp.exp(-jnp.abs(logit)))
     factor = jnp.exp(log_sig / forgetting_softness - boost[...])
-    high = factor.astype(BF16).astype(F32)
-    middle = (factor - high).astype(BF16).astype(F32)
-    low = factor - high - middle
-    steps = seqs // STEP
-    for i in range(steps):
-        cut = slice(i * STEP, (i + 1) * STEP)
-        fkq_ref[i, 0:STEP] = high[cut]
-        fkq_ref[i, STEP : 2 * STEP] = middle[cut]
-        fkq_ref[i, 2 * STEP : 3 * STEP] = low[cut]
-        fkq_ref[i, 5 * STEP : 6 * STEP] = jnp.zeros_like(low[cut])
+
+    def fill(first, value):
+        for i in range(steps):
+            lines[i, first : first + STEP] = value[i * STEP : (i + 1) * STEP]
+
+    def fill_exact(first, value):
+        high = value.astype(BF16).astype(F32)
+        middle = (value - high).astype(BF16).astype(F32)
+        fill(first, high)
+        fill(first + STEP, middle)
+        fill(first + 2 * STEP, value - high - middle)
+
+    fill_exact(0, factor)
+    fill(7 * STEP, jnp.zeros_like(factor))
+    line = lax.broadcasted_iota(jnp.int32, spots.shape, 0)
+    block = lax.broadcasted_iota(jnp.int32, spots.shape, 1) // KEY_CHANNELS
+    band = line // STEP
+    kind = (band >= 3).astype(jnp.int32) + (band >= 4).astype(jnp.int32)
+    wanted = (block // STEP == kind) & (block % STEP == line % STEP) & (band < 7)
+    spots[...] = wanted.astype(F32).astype(BF16)
+
     cuts = [(0, 2 * span), (2 * span, width), (2 * span + width, width)]
     needs = [(0, 1), (2,), (3,)]
-    copies = list(sent) + list(pushes)
 
     def cut_of(ref, b, *lead):
         return ref.at[(*lead, slice(None), pl.ds(*cuts[b]))]
 
-    def ready(b):
+    def expect(target, sem):
+        pltpu.make_async_remote_copy(
+            src_ref=target,
+            dst_ref=target,
+            send_sem=sem,
+            recv_sem=sem,
+            device_id=partner,
+            device_id_type=MESH,
+        ).wait_recv()
+
+    def prepare(b):
         for i in needs[b]:
             loads[i].wait()
             pushes[i].wait_recv()
@@ -370,21 +433,12 @@
         )
 
     def arrival(there):
-        return pltpu.make_async_remote_copy(
-            src_ref=chunks.at[0],
-            dst_ref=spread.at[there],
-            send_sem=chunk_send.at[0],
-            recv_sem=chunk_recv.at[there],
-            device_id=partner,
-            device_id_type=MESH,
-        )
-
-    arrival(near).wait_recv()
-    for b in range(3):
-        ready(b)
+        expect(spread.at[there], chunk_recv.at[there])
+
+    def to_near(b):
         start, size = cuts[b]
         near_out[:, start : start + size] = part_of(near, b).astype(BF16)
-        copies.append(
+        done.append(
             send(
                 cut_of(near_out, b),
                 cut_of(near_in, b),
@@ -393,8 +447,8 @@
                 {"ep": near * 2 + core},
             )
         )
-    arrival(inner_there).wait_recv()
-    for b in range(3):
+
+    def to_inner(b):
         start, size = cuts[b]
         part = part_of(inner_there, b)
         held[:, start : start + size] = part
@@ -410,12 +464,12 @@
                 {"ep": near * 2 + core},
             )
 
-    arrival(outer_there).wait_recv()
     slot = jnp.where(inside, 0, 1)
-    for b in range(3):
+
+    def to_outer(b):
         start, size = cuts[b]
         far_out[:, start : start + size] = part_of(outer_there, b).astype(BF16)
-        copies.append(
+        done.append(
             send(
                 cut_of(far_out, b),
                 cut_of(far_in, b, slot),
@@ -435,199 +489,128 @@
             device_id_type=MESH,
         )
 
-    def waiting(target, b, sem):
-        return pltpu.make_async_remote_copy(
-            src_ref=cut_of(mid_out, b),
-            dst_ref=target,
-            send_sem=mid_send.at[b],
-            recv_sem=sem,
-            device_id=partner,
-            device_id_type=MESH,
-        )
-
-    @pl.when(inside)
-    def _():
-        for b in range(3):
-            start, size = cuts[b]
-            waiting(cut_of(mid_in, b), b, mid_recv.at[b]).wait_recv()
+    def merge(b):
+        start, size = cuts[b]
+
+        @pl.when(inside)
+        def _():
+            expect(cut_of(mid_in, b), mid_recv.at[b])
             merged = held[:, start : start + size] + mid_in[:, start : start + size].astype(F32)
             mid_out[:, start : start + size] = merged.astype(BF16)
             middle_copy(b).start()
 
-    for b in range(3):
+        held[:, start : start + size] = part_of(row, b)
+
+    def total_of(b):
         start, size = cuts[b]
-        held[:, start : start + size] = part_of(row, b)
-    for b in range(3):
-        start, size = cuts[b]
-        waiting(cut_of(near_in, b), b, near_recv.at[b]).wait_recv()
-        waiting(cut_of(far_in, b, 0), b, far_recv.at[0, b]).wait_recv()
+        expect(cut_of(near_in, b), near_recv.at[b])
+        expect(cut_of(far_in, b, 0), far_recv.at[0, b])
         held[:, start : start + size] += near_in[:, start : start + size].astype(F32) + far_in[
             0, :, start : start + size
         ].astype(F32)
 
         @pl.when(jnp.logical_not(inside))
         def _():
-            waiting(cut_of(far_in, b, 1), b, far_recv.at[1, b]).wait_recv()
+            expect(cut_of(far_in, b, 1), far_recv.at[1, b])
             held[:, start : start + size] += far_in[1, :, start : start + size].astype(F32)
 
-        total = held[:, start : start + size]
-        if b == 0:
-            query = (total[:, :span] * KEY_CHANNELS ** (-0.5)).astype(BF16).astype(F32)
-            key = total[:, span:].astype(BF16).astype(F32)
-            for i in range(steps):
-                cut = slice(i * STEP, (i + 1) * STEP)
-                fkq_ref[i, 3 * STEP : 4 * STEP] = key[cut]
-                fkq_ref[i, 4 * STEP : 5 * STEP] = query[cut]
-        else:
-            target = value_ref if b == 1 else gate_ref
-            total = total.astype(BF16).astype(F32)
-            for i in range(steps):
-                target[i] = total[i * STEP : (i + 1) * STEP]
-    for copy in copies:
-        copy.wait_send()
-    for b in range(3):
-        middle_copy(b).wait_send()
-    for load in later:
-        load.wait()
-
-
-def state_kernel(state_ref, fkq_ref, value_ref, new_hbm, read_ref, spots, wide, buffer, out_sem):
-    seqs, _, width = state_ref.shape
-    heads = width // DV
-    steps = seqs // STEP
-    lines = fkq_ref.shape[1]
-    line = lax.broadcasted_iota(jnp.int32, (lines, 3 * STEP * KEY_CHANNELS), 0)
-    block = lax.broadcasted_iota(jnp.int32, (lines, 3 * STEP * KEY_CHANNELS), 1) // KEY_CHANNELS
-    kind = jnp.maximum(line // STEP - 2, 0)
-    wanted = (block // STEP == kind) & (block % STEP == line % STEP) & (line < 5 * STEP)
-    spots[...] = wanted.astype(F32).astype(BF16)
-
-    def flush(s):
-        return pltpu.make_async_copy(buffer.at[s], new_hbm.at[s], out_sem.at[s])
+        return held[:, start : start + size]
+
+    arrival(near)
+    prepare(0)
+    to_near(0)
+    state_load.start()
+    arrival(inner_there)
+    to_inner(0)
+    arrival(outer_there)
+    to_outer(0)
+    prepare(1)
+    to_inner(1)
+    to_outer(1)
+    to_near(1)
+    out_load.start()
+    merge(0)
+    prepare(2)
+    to_inner(2)
+    to_outer(2)
+    to_near(2)
+    for load in expert_loads:
+        load.start()
+    pushes.append(
+        send(expert_down_hbm.at[0], pair_down, push_send.at[4], push_recv.at[4], partner)
+    )
+    merge(1)
+    merge(2)
+    total = total_of(0)
+    query = (total[:, :span] * KEY_CHANNELS ** (-0.5)).astype(BF16).astype(F32)
+    key = total[:, span:].astype(BF16).astype(F32)
+    fill(3 * STEP, key)
+    fill_exact(4 * STEP, query * factor)
+    alike = query * key
+    state_load.wait()
 
     @pl.loop(0, steps)
     def _(i):
         for h in range(heads):
-            turned = fkq_ref[i, :, h * KEY_CHANNELS : (h + 1) * KEY_CHANNELS].T.astype(BF16)
-            wide[h] = jnp.dot(turned, spots[...], preferred_element_type=F32)
+            flat = lines[i, :, h * KEY_CHANNELS : (h + 1) * KEY_CHANNELS].T.astype(BF16)
+            turned[i, h] = flat
+            wide[h, :, 0 : STEP * KEY_CHANNELS] = jnp.dot(
+                flat, spots[:, 2 * STEP * KEY_CHANNELS :], preferred_element_type=F32
+            )
         for s in range(STEP):
             sums = []
             for h in range(heads):
-                factor, key, query = (
+                weight = wide[h, :, s * KEY_CHANNELS : (s + 1) * KEY_CHANNELS]
+                for g in range(DV // KEY_CHANNELS):
+                    start = h * DV + g * KEY_CHANNELS
+                    old = state_ref[i * STEP + s, :, start : start + KEY_CHANNELS]
+                    sums.append(jnp.sum((weight * old).reshape(-1, 8, KEY_CHANNELS), axis=0))
+            read[i * STEP + s] = jnp.concatenate(sums, axis=1)
+
+    def renew(i):
+        for h in range(heads):
+            wide[h] = jnp.dot(
+                turned[i, h], spots[:, : 2 * STEP * KEY_CHANNELS], preferred_element_type=F32
+            )
+        for s in range(STEP):
+            for h in range(heads):
+                keep, add = (
                     wide[h, :, (j * STEP + s) * KEY_CHANNELS : (j * STEP + s + 1) * KEY_CHANNELS]
-                    for j in range(3)
+                    for j in range(2)
                 )
                 for g in range(DV // KEY_CHANNELS):
                     start = h * DV + g * KEY_CHANNELS
-                    lanes = slice(start, start + KEY_CHANNELS)
-                    updated = factor * state_ref[i * STEP + s, :, lanes] + key * value_ref[
-                        i, s : s + 1, lanes
-                    ]
-                    buffer[i * STEP + s, :, lanes] = updated
-                    sums.append(jnp.sum((query * updated).reshape(-1, 8, KEY_CHANNELS), axis=0))
-            read_ref[i * STEP + s] = jnp.concatenate(sums, axis=1)
-            flush(i * STEP + s).start()
-
-    for s in range(seqs):
-        flush(s).wait()
-
-
-def mixture_kernel(
-    n,
-    m,
-    read_ref,
-    rows_ref,
-    head_gain_ref,
-    stream_hbm,
-    gain_ref,
-    index_ref,
-    score_ref,
-    prob_ref,
-    w_out,
-    w_gate,
-    w_up,
-    w_down,
-    out_ref,
-    own_stream,
-    lhs,
-    part_out,
-    part_in,
-    slots_out,
-    shares_out,
-    shares_in,
-    arrived,
-    hidden_out,
-    hidden_in,
-    pair_down,
-    ready,
-    returned,
-    load_sem,
-    part_send,
-    part_recv,
-    slot_send,
-    slot_recv,
-    share_send,
-    share_recv,
-    join_send,
-    join_recv,
-    swap_send,
-    swap_recv,
-    push_send,
-    push_recv,
-    hid_send,
-    hid_recv,
-    back_send,
-    back_recv,
-):
-    me = lax.axis_index("ep")
-    tp = lax.axis_index("tp")
-    core = lax.rem(me, 2)
-    row = me // 2
-    rows = n // 2
-    seqs, width = own_stream.shape
-    capacity = slots_out.shape[1]
-    half = rows * capacity
-    inner = w_gate.shape[1]
-    tps = [m - 1 - tp, tp + 1 - 2 * lax.rem(tp, 2), lax.rem(tp + 2, m)]
-    near = row + 1 - 2 * lax.rem(row, 2)
-    zs = [3 - row, 3 - near, near]
-    other = me + 1 - 2 * core
-    partners = (
-        [{"tp": t} for t in tps]
-        + [{"ep": z * 2 + core} for z in zs]
-        + [{"ep": other}]
-        + [{"tp": t, "ep": other} for t in tps]
-    )
-    barrier = pltpu.get_barrier_semaphore()
-    for partner in partners:
-        pl.semaphore_signal(barrier, inc=1, device_id=partner, device_id_type=MESH)
-    own_cut = pl.ds(pl.multiple_of(tp * width, 128), width)
-    load = pltpu.make_async_copy(stream_hbm.at[:, own_cut], own_stream, load_sem.at[0])
-    load.start()
-    for i in range(seqs // STEP):
-        lhs[i * STEP : (i + 1) * STEP] = rows_ref[i]
-    gates = lhs[...]
+                    cut = slice(start, start + KEY_CHANNELS)
+                    state_ref[i * STEP + s, :, cut] = (
+                        keep * state_ref[i * STEP + s, :, cut]
+                        + add * values[i * STEP + s : i * STEP + s + 1, cut]
+                    )
+
+    values[...] = total_of(1).astype(BF16).astype(F32)
+    readout = jnp.sum(read[...], axis=1)
+    gates = total_of(2).astype(BF16).astype(F32)
     silu = gates / (1.0 + jnp.exp(-gates))
-    readout = jnp.sum(read_ref[...], axis=1)
-    for h in range(width // DV):
-        lanes = slice(h * DV, (h + 1) * DV)
-        part = readout[:, lanes]
+    for load in tables:
+        load.wait()
+    for h in range(heads):
+        cut = slice(h * DV, (h + 1) * DV)
+        same = jnp.sum(
+            alike[:, h * KEY_CHANNELS : (h + 1) * KEY_CHANNELS], axis=-1, keepdims=True
+        )
+        part = readout[:, cut] + same * values[:, cut]
         mean_sq = jnp.mean(part * part, axis=-1, keepdims=True)
-        lhs[:, lanes] = part * lax.rsqrt(mean_sq + epsilon) * head_gain_ref[...] * silu[:, lanes]
-    gated = lhs[...].astype(BF16)
-    done = []
+        held[:, cut] = part * lax.rsqrt(mean_sq + epsilon) * head_gain_ref[...] * silu[:, cut]
+    gated = held[:, :width].astype(BF16)
     parts = []
+    out_load.wait()
     for j, there in enumerate(tps + [tp]):
         cut = pl.ds(pl.multiple_of(there * width, 128), width)
         part = jnp.dot(gated, w_out[:, cut], preferred_element_type=F32)
-        if j == 0:
-            pl.semaphore_wait(barrier, len(partners))
         if j < m - 1:
             part_out[j] = part.astype(BF16)
             parts.append(
                 send(part_out.at[j], part_in.at[j], part_send.at[j], part_recv.at[j], {"tp": there})
             )
-    push = send(w_down.at[0], pair_down, push_send.at[0], push_recv.at[0], {"ep": other})
 
     index = index_ref[...]
     group = index[0:1] // 2
@@ -646,7 +629,6 @@
     table = jnp.zeros((128, seqs), F32)
     for k in range(index.shape[0]):
         table += jnp.where(place_line == lax.rem(index[k : k + 1], 2), shares[k : k + 1], 0.0)
-    nt = (((1,), (1,)), ((), ()))
     shares_out[...] = lax.dot_general(
         placing, table, nt, preferred_element_type=F32, precision=lax.Precision.HIGHEST
     ).reshape(GROUPS, capacity, 128)
@@ -663,8 +645,9 @@
             )
         )
     shares_in[row] = shares_out[row]
-    load.wait()
-    total = part + own_stream[...].astype(F32)
+    renew(0)
+    own_cut = pl.ds(pl.multiple_of(tp * width, 128), width)
+    total = part + stream[:, own_cut].astype(F32)
     for j in (1, 2, 0):
         parts[j].wait_recv()
         total = total + part_in[j].astype(F32)
@@ -707,16 +690,6 @@
             )
         swap(tp, z)
 
-    def expect(target, sem):
-        pltpu.make_async_remote_copy(
-            src_ref=target,
-            dst_ref=target,
-            send_sem=sem,
-            recv_sem=sem,
-            device_id={"ep": other},
-            device_id_type=MESH,
-        ).wait_recv()
-
     def relay(z):
         for t in (tps[1], tps[2], tps[0]):
             expect(arrived.at[t, core, z], join_recv.at[t, z])
@@ -724,6 +697,7 @@
 
     order = [row] + zs[::-1]
     join(row)
+    renew(1)
     expect(arrived.at[tp, core, order[1]], slot_recv.at[order[1]])
     join(order[1])
     expect(arrived.at[tp, core, order[2]], slot_recv.at[order[2]])
@@ -731,8 +705,11 @@
     relay(order[0])
     expect(arrived.at[tp, core, order[3]], slot_recv.at[order[3]])
     join(order[3])
+    renew(2)
     relay(order[1])
     relay(order[2])
+    for load in expert_loads:
+        load.wait()
 
     tokens_held = n * capacity
     square = jnp.zeros((tokens_held, 1), F32)
@@ -776,16 +753,17 @@
         )
     )
     hidden_in[core, tp] = hidden_out[core]
-    push.wait_recv()
+    renew(3)
+    pushes[4].wait_recv()
     own_sum = jnp.zeros((half, width), F32)
     pair_sum = jnp.zeros((half, width), F32)
     for j, t in enumerate([tp, tps[1], tps[2], tps[0]]):
-        lines = pl.ds(pl.multiple_of(t * inner, 128), inner)
+        band = pl.ds(pl.multiple_of(t * inner, 128), inner)
         if j > 0:
             expect(hidden_in.at[core, t], hid_recv.at[core, t])
-        own_sum += jnp.dot(hidden_in[core, t], w_down[0, lines, :], preferred_element_type=F32)
+        own_sum += jnp.dot(hidden_in[core, t], w_down[0, band, :], preferred_element_type=F32)
         expect(hidden_in.at[1 - core, t], hid_recv.at[1 - core, t])
-        pair_sum += jnp.dot(hidden_in[1 - core, t], pair_down[lines, :], preferred_element_type=F32)
+        pair_sum += jnp.dot(hidden_in[1 - core, t], pair_down[band, :], preferred_element_type=F32)
     for z in zs:
         expect(shares_in.at[z], share_recv.at[z])
     share = shares_in[...].reshape(half, 128)
@@ -816,8 +794,10 @@
         preferred_element_type=F32,
     )
     out_ref[...] = (mixed.astype(F32) + mixture).astype(BF16)
-    for copy in parts + done + [push]:
+    for copy in parts + done + pushes:
         copy.wait_send()
+    for b in range(3):
+        middle_copy(b).wait_send()
 
 
 def fused(
@@ -851,27 +831,42 @@
     steps = seqs // STEP
     total = 2 * span + 2 * width
     rows = n // 2
+    inner = expert_gate_weight.shape[1]
+    capacity = 2 * seqs * expert_index_table.shape[1] // n
+    lines = 8 * STEP
     dma = pltpu.SemaphoreType.DMA
     vmem = pl.BlockSpec(memory_space=pltpu.VMEM)
     hbm = pl.BlockSpec(memory_space=pltpu.HBM)
-    ahead = (
+    operands = (
+        stream,
+        mixer_norm_gain.reshape(1, model),
+        query_matrix,
+        key_matrix,
+        value_matrix,
+        output_gate_weight,
+        decay_lower_factor.T,
+        decay_upper_factor,
+        forgetting_boost,
+        head_norm_gain.reshape(1, DV),
+        mixture_norm_gain.reshape(1, model),
+        expert_index_table.T,
+        expert_scores_within.T,
+        group_probability.reshape(1, seqs),
         previous_state,
         output_matrix,
         expert_gate_weight,
         expert_up_weight,
         expert_down_weight,
     )
-    fkq, values, gates, *held = pl.pallas_call(
-        functools.partial(project_kernel, n),
-        name="project",
+    new_state, new_stream = pl.pallas_call(
+        functools.partial(layer_kernel, n, m),
+        name="layer",
         out_shape=(
-            jax.ShapeDtypeStruct((steps, 6 * STEP, span), F32),
-            jax.ShapeDtypeStruct((steps, STEP, width), F32),
-            jax.ShapeDtypeStruct((steps, STEP, width), F32),
-            *(pltpu.VMEM(a.shape, a.dtype) for a in ahead),
+            pltpu.VMEM(previous_state.shape, F32),
+            jax.ShapeDtypeStruct((seqs, width), BF16),
         ),
-        in_specs=[hbm] * (9 + len(ahead)),
-        out_specs=(vmem,) * (3 + len(ahead)),
+        in_specs=[hbm] * len(operands),
+        out_specs=(vmem, vmem),
         scratch_shapes=[
             pltpu.VMEM((seqs, model), BF16),
             pltpu.VMEM((1, model), F32),
@@ -879,6 +874,16 @@
             pltpu.VMEM((rank, model), BF16),
             pltpu.VMEM((rank, span), BF16),
             pltpu.VMEM((seqs, span), F32),
+            pltpu.VMEM((1, DV), F32),
+            pltpu.VMEM((1, model), F32),
+            pltpu.VMEM(expert_index_table.shape[::-1], jnp.int32),
+            pltpu.VMEM(expert_scores_within.shape[::-1], F32),
+            pltpu.VMEM((1, seqs), F32),
+            pltpu.VMEM(output_matrix.shape, BF16),
+            pltpu.VMEM(expert_gate_weight.shape, BF16),
+            pltpu.VMEM(expert_up_weight.shape, BF16),
+            pltpu.VMEM(expert_down_weight.shape, BF16),
+            pltpu.VMEM(expert_down_weight.shape[1:], BF16),
             pltpu.VMEM((rows, seqs, 2 * feats), BF16),
             pltpu.VMEM((rows, seqs, 2 * feats), BF16),
             pltpu.VMEM((seqs, total), BF16),
@@ -888,9 +893,25 @@
             pltpu.VMEM((seqs, total), BF16),
             pltpu.VMEM((2, seqs, total), BF16),
             pltpu.VMEM((seqs, total), F32),
-            dma((14,)),
-            dma((4,)),
-            dma((4,)),
+            pltpu.VMEM((steps, lines, span), F32),
+            pltpu.VMEM((steps, width // DV, KEY_CHANNELS, lines), BF16),
+            pltpu.VMEM((lines, 3 * STEP * KEY_CHANNELS), BF16),
+            pltpu.VMEM((width // DV, KEY_CHANNELS, 2 * STEP * KEY_CHANNELS), F32),
+            pltpu.VMEM((seqs, width), F32),
+            pltpu.VMEM((seqs, 8, width), F32),
+            pltpu.VMEM((m - 1, seqs, width), BF16),
+            pltpu.VMEM((m - 1, seqs, width), BF16),
+            pltpu.VMEM((GROUPS, capacity, width), BF16),
+            pltpu.VMEM((GROUPS, capacity, 128), F32),
+            pltpu.VMEM((GROUPS, capacity, 128), F32),
+            pltpu.VMEM((m, 2, rows, capacity, width), BF16),
+            pltpu.VMEM((2, rows * capacity, inner), BF16),
+            pltpu.VMEM((2, m, rows * capacity, inner), BF16),
+            pltpu.VMEM((rows, capacity, width), BF16),
+            pltpu.VMEM((rows, capacity, width), BF16),
+            dma((len(operands),)),
+            dma((5,)),
+            dma((5,)),
             dma((rows,)),
             dma((rows,)),
             dma((3,)),
@@ -899,69 +920,6 @@
             dma((3,)),
             dma((3,)),
             dma((2, 3)),
-        ],
-        compiler_params=pltpu.CompilerParams(
-            collective_id=0, has_side_effects=True, vmem_limit_bytes=12 * 2**20
-        ),
-        cost_estimate=pl.CostEstimate(flops=COST, bytes_accessed=3 * feats * total, transcendentals=0),
-    )(
-        *(pltpu.with_memory_space_constraint(a, pltpu.HBM) for a in (
-            stream,
-            mixer_norm_gain.reshape(1, model),
-            query_matrix,
-            key_matrix,
-            value_matrix,
-            output_gate_weight,
-            decay_lower_factor.T,
-            decay_upper_factor,
-            forgetting_boost,
-            *ahead,
-        ))
-    )
-    previous_state, output_matrix, expert_gate_weight, expert_up_weight, expert_down_weight = held
-    new_state, readout = pl.pallas_call(
-        state_kernel,
-        name="state",
-        out_shape=(
-            jax.ShapeDtypeStruct(previous_state.shape, F32),
-            jax.ShapeDtypeStruct((seqs, 8, width), F32),
-        ),
-        in_specs=[vmem, vmem, vmem],
-        out_specs=(hbm, vmem),
-        scratch_shapes=[
-            pltpu.VMEM((6 * STEP, 3 * STEP * KEY_CHANNELS), BF16),
-            pltpu.VMEM((width // DV, KEY_CHANNELS, 3 * STEP * KEY_CHANNELS), F32),
-            pltpu.VMEM(previous_state.shape, F32),
-            dma((seqs,)),
-        ],
-        compiler_params=pltpu.CompilerParams(vmem_limit_bytes=14 * 2**20),
-        cost_estimate=pl.CostEstimate(
-            flops=COST // 4, bytes_accessed=4 * previous_state.size, transcendentals=0
-        ),
-    )(previous_state, fkq, values)
-    inner = expert_gate_weight.shape[1]
-    capacity = 2 * seqs * expert_index_table.shape[1] // n
-    new_stream = pl.pallas_call(
-        functools.partial(mixture_kernel, n, m),
-        name="mixture",
-        out_shape=jax.ShapeDtypeStruct((seqs, width), BF16),
-        in_specs=[vmem] * 3 + [hbm] + [vmem] * 8,
-        out_specs=vmem,
-        scratch_shapes=[
-            pltpu.VMEM((seqs, width), BF16),
-            pltpu.VMEM((seqs, width), F32),
-            pltpu.VMEM((m - 1, seqs, width), BF16),
-            pltpu.VMEM((m - 1, seqs, width), BF16),
-            pltpu.VMEM((GROUPS, capacity, width), BF16),
-            pltpu.VMEM((GROUPS, capacity, 128), F32),
-            pltpu.VMEM((GROUPS, capacity, 128), F32),
-            pltpu.VMEM((m, 2, rows, capacity, width), BF16),
-            pltpu.VMEM((2, rows * capacity, inner), BF16),
-            pltpu.VMEM((2, m, rows * capacity, inner), BF16),
-            pltpu.VMEM(expert_down_weight.shape[1:], BF16),
-            pltpu.VMEM((rows, capacity, width), BF16),
-            pltpu.VMEM((rows, capacity, width), BF16),
-            dma((1,)),
             dma((m - 1,)),
             dma((m - 1,)),
             dma((rows,)),
@@ -972,31 +930,18 @@
             dma((m, rows)),
             dma((m, rows)),
             dma((m, rows)),
-            dma((1,)),
-            dma((1,)),
             dma((2 * m - 1,)),
             dma((2, m)),
             dma((rows,)),
             dma((rows,)),
         ],
         compiler_params=pltpu.CompilerParams(
-            collective_id=1, has_side_effects=True, vmem_limit_bytes=VM3 * 2**20
+            collective_id=0, has_side_effects=True, vmem_limit_bytes=GRANT * 2**20
         ),
-        cost_estimate=pl.CostEstimate(flops=COST, bytes_accessed=2 * output_matrix.size, transcendentals=0),
-    )(
-        readout,
-        gates,
-        head_norm_gain.reshape(1, DV),
-        stream,
-        mixture_norm_gain.reshape(1, model),
-        expert_index_table.T,
-        expert_scores_within.T,
-        group_probability.reshape(1, seqs),
-        output_matrix,
-        expert_gate_weight,
-        expert_up_weight,
-        expert_down_weight,
-    )
+        cost_estimate=pl.CostEstimate(
+            flops=COST, bytes_accessed=4 * previous_state.size, transcendentals=0
+        ),
+    )(*(pltpu.with_memory_space_constraint(a, pltpu.HBM) for a in operands))
     return (new_stream, new_state)
 
 

time: 51.7 us -> 47.3 us (0.915)
  Pallas kernels: 50.2 us -> 42.5 us
  local copies, waits for them, and re-layouts: 0.66 us -> 4.01 us
    pallas_call x3 -> x1, Pallas kernels: 50.2 us -> 42.5 us  [fused(): pl.pallas_call(functools.partial(layer_kernel, n, m), name='layer', out_s...]
    unnamed x13 -> x2, local copies, waits for them, and re-layouts: 0.66 us -> 4.01 us
where the time goes in v2:
time: 47.3 us; the launch traced here: 47.2 us
  Pallas kernels  42.5 us (90%)
  local copies, waits for them, and re-layouts  4.01 us (8%)
  between operations  0.65 us (1%)
    pallas_call x1, Pallas kernels, fused(): pl.pallas_call(functools.partial(layer_kernel, n, m), name='layer', out_s...  42.5 us
    unnamed x2, local copies, waits for them, and re-layouts  4.01 us

profile of v2, /device:TPU:0, one launch (start us, length us, event | category | flops | bytes accessed | tf_op | source)
XLA Modules:
  0.0 47.2 jit_solution(1768302019539008945)
XLA Ops:
  0.6 42.5 %layer.1 = (f32[16,128,1024]{2,1,0:T(8,128)S(1)}, bf16[16,1024]{1,0:T(8,128)(2,1)S(1)}) custom-call(bf16[16,4096]{1,0:T(8,128)(2,1)} %stream_hbm.1, f32[1,4096]{1,0:T(1,128)} %bitcast.8, bf16[512,2048]{1,0:T(8,128)(2,1)} %query_hbm.1, bf16[512,2048]{1,0:T(8,128)(2,1)} %key_hbm.1, bf16[512,1024]{1,0:T(8,128)(2,1)} %value_hbm.1, bf16[512,1024]{1,0:T(8,128)(2,1)} %gate_hbm.1, ...), custom_call_target="tpu_custom_call" | custom-call | flops 20000000000 | bytes 8388608 | tf_op jit(solution)/shard_map/layer/pallas_call | solution.py:861
  43.1 3.4 %copy.23 = f32[16,128,1024]{2,1,0:T(8,128)} copy(f32[16,128,1024]{2,1,0:T(8,128)S(1)} %get-tuple-element.7) | data formatting | bytes 16777216
  46.5 0.6 %copy.24 = bf16[16,1024]{1,0:T(8,128)(2,1)} copy(bf16[16,1024]{1,0:T(8,128)(2,1)S(1)} %get-tuple-element.10) | data formatting | bytes 65536

commit v3 on v2

--- a/solution.py
+++ b/solution.py
@@ -228,8 +228,7 @@
     score_ref,
     prob_ref,
     w_out,
-    w_gate,
-    w_up,
+    w_in,
     w_down,
     pair_down,
     chunks,
@@ -296,7 +295,7 @@
     steps = seqs // STEP
     capacity = slots_out.shape[1]
     half = rows * capacity
-    inner = w_gate.shape[1]
+    inner = w_in.shape[1]
     nt = (((1,), (1,)), ((), ()))
     side = row // 2
     inside = lax.rem(row, 2) != side
@@ -340,8 +339,8 @@
         (prob_hbm, prob_ref),
         (state_hbm, state_ref),
         (output_hbm, w_out),
-        (expert_gate_hbm, w_gate),
-        (expert_up_hbm, w_up),
+        (expert_gate_hbm.at[0], w_in.at[0]),
+        (expert_up_hbm.at[0], w_in.at[1]),
         (expert_down_hbm, w_down),
     ]
     copies = [
@@ -374,10 +373,15 @@
                 {"ep": there * 2 + core},
             )
         )
-    pushes = [
-        send(source, place, push_send.at[i], push_recv.at[i], partner)
-        for i, (source, place) in enumerate(zip(sources, places))
-    ]
+
+    def push(i):
+        pushes.append(
+            send(sources[i], places[i], push_send.at[i], push_recv.at[i], partner)
+        )
+
+    pushes = []
+    for i in range(3):
+        push(i)
     for load in copies[2:5]:
         load.wait()
     low_rank = lax.dot_general(normed, lower[...], nt, preferred_element_type=F32).astype(BF16)
@@ -524,6 +528,7 @@
     to_inner(0)
     arrival(outer_there)
     to_outer(0)
+    push(3)
     prepare(1)
     to_inner(1)
     to_outer(1)
@@ -713,8 +718,7 @@
 
     tokens_held = n * capacity
     square = jnp.zeros((tokens_held, 1), F32)
-    gate_pre = jnp.zeros((tokens_held, inner), F32)
-    up_pre = jnp.zeros((tokens_held, inner), F32)
+    before = jnp.zeros((tokens_held, 2 * inner), F32)
     for j, t in enumerate([tp, tps[1], tps[2], tps[0]]):
         if j == 1:
             relay(order[3])
@@ -724,11 +728,12 @@
         tokens = arrived[t].astype(F32).reshape(tokens_held, width)
         square += jnp.sum(tokens * tokens, axis=-1, keepdims=True)
         scaled = (tokens * gain_ref[:, cut]).astype(BF16)
-        gate_pre += lax.dot_general(scaled, w_gate[0, :, cut], nt, preferred_element_type=F32)
-        up_pre += lax.dot_general(scaled, w_up[0, :, cut], nt, preferred_element_type=F32)
+        before += lax.dot_general(
+            scaled, w_in[:, :, cut].reshape(2 * inner, width), nt, preferred_element_type=F32
+        )
     scale = lax.rsqrt(square / (m * width) + epsilon)
-    gate_pre *= scale
-    up_pre *= scale
+    gate_pre = before[:, :inner] * scale
+    up_pre = before[:, inner:] * scale
     hidden_out[...] = (
         (gate_pre / (1.0 + jnp.exp(-gate_pre)) * up_pre).astype(BF16).reshape(2, half, inner)
     )
@@ -880,8 +885,7 @@
             pltpu.VMEM(expert_scores_within.shape[::-1], F32),
             pltpu.VMEM((1, seqs), F32),
             pltpu.VMEM(output_matrix.shape, BF16),
-            pltpu.VMEM(expert_gate_weight.shape, BF16),
-            pltpu.VMEM(expert_up_weight.shape, BF16),
+            pltpu.VMEM((2, *expert_gate_weight.shape[1:]), BF16),
             pltpu.VMEM(expert_down_weight.shape, BF16),
             pltpu.VMEM(expert_down_weight.shape[1:], BF16),
             pltpu.VMEM((rows, seqs, 2 * feats), BF16),

time: 47.3 us -> 47 us (level)
  no operation moved by 1% of the time
where the time goes in v3:
time: 47 us; the launch traced here: 46.8 us
  Pallas kernels  42.1 us (90%)
  local copies, waits for them, and re-layouts  4.01 us (9%)
  between operations  0.65 us (1%)
    pallas_call x1, Pallas kernels, fused(): pl.pallas_call(functools.partial(layer_kernel, n, m), name='layer', out_s...  42.1 us
    unnamed x2, local copies, waits for them, and re-layouts  4.01 us

profile of v3, /device:TPU:0, one launch (start us, length us, event | category | flops | bytes accessed | tf_op | source)
XLA Modules:
  0.0 46.8 jit_solution(11904512417113911949)
XLA Ops:
  0.6 42.1 %layer.1 = (f32[16,128,1024]{2,1,0:T(8,128)S(1)}, bf16[16,1024]{1,0:T(8,128)(2,1)S(1)}) custom-call(bf16[16,4096]{1,0:T(8,128)(2,1)} %stream_hbm.1, f32[1,4096]{1,0:T(1,128)} %bitcast.8, bf16[512,2048]{1,0:T(8,128)(2,1)} %query_hbm.1, bf16[512,2048]{1,0:T(8,128)(2,1)} %key_hbm.1, bf16[512,1024]{1,0:T(8,128)(2,1)} %value_hbm.1, bf16[512,1024]{1,0:T(8,128)(2,1)} %gate_hbm.1, ...), custom_call_target="tpu_custom_call" | custom-call | flops 20000000000 | bytes 8388608 | tf_op jit(solution)/shard_map/layer/pallas_call | solution.py:866
  42.8 3.4 %copy.23 = f32[16,128,1024]{2,1,0:T(8,128)} copy(f32[16,128,1024]{2,1,0:T(8,128)S(1)} %get-tuple-element.7) | data formatting | bytes 16777216
  46.2 0.6 %copy.24 = bf16[16,1024]{1,0:T(8,128)(2,1)} copy(bf16[16,1024]{1,0:T(8,128)(2,1)S(1)} %get-tuple-element.10) | data formatting | bytes 65536
